TPU v7x, 256 devices: a whole 4x4x8 slice. The times are simulated.
256 devices in a mesh: sp: 64 (over z, y, core), tp: 4 (over x).
Axes of the slice: x: 4, y: 4, z: 8, core: 2. Of those that a mesh axis runs over, the one named last changes fastest.
Arguments:
- stream_in: bfloat16 [16384, 2048], P(('sp', 'tp')), may hold values from -6 to 6
- queries_one: bfloat16 [16384, 1024], P('sp', 'tp'), may hold values from -120 to 120
- queries_two: bfloat16 [16384, 1024], P('sp', 'tp'), may hold values from -120 to 120
- keys_one: bfloat16 [16384, 512], P('sp', 'tp'), may hold values from -7 to 7
- keys_two: bfloat16 [16384, 512], P('sp', 'tp'), may hold values from -7 to 7
- values: bfloat16 [16384, 1024], P('sp', 'tp'), may hold values from -6 to 6
- lambdas: float32 [8], P('tp'), may hold values from 0.3 to 0.8
- head_gain: float32 [256], replicated, may hold values from 0.1 to 1.9
- out_weight: bfloat16 [2048, 2048], P('tp'), may hold values from -0.125 to 0.125
- norm_gain: float32 [2048], replicated, may hold values from 0.1 to 1.9
- expert_ids: int32 [16384, 2], P(('sp', 'tp')), may hold values from 0 to 63, all different within a row; in each aligned block of 64 rows (0 to 63, 64 to 127, ...) at most 4 rows name the same one
- route_weight: float32 [16384, 2], P(('sp', 'tp')), may hold values from 0.1 to 1
- gate_weight: bfloat16 [64, 2048, 1024], P('sp', None, 'tp'), may hold values from -0.125 to 0.125
- up_weight: bfloat16 [64, 2048, 1024], P('sp', None, 'tp'), may hold values from -0.125 to 0.125
- down_weight: bfloat16 [64, 1024, 2048], P('sp', 'tp'), may hold values from -0.1875 to 0.1875
Outputs:
- mixed: bfloat16 [16384, 2048], P(('sp', 'tp'))
Inputs may be any that keep to these rules, and one draw needn't show every extreme that they name: `expert_ids`: each row names 2 different experts. In each aligned block of 64 rows no expert is named more than 4 times, a bound that some block reaches.
All inputs are finite; a program needn't handle non-finite values.
Results may differ from a plain program's by a relative error of at most 0.013.
Values may be sent and summed in bfloat16 or wider, within the bound.
A program may use at most 128 MiB of HBM per device.

v0:
```python
import math

import jax
import jax.numpy as jnp
from jax import lax
from jax.sharding import PartitionSpec as P

HEAD_DIM = 128
VAL_DIM = 256


EPS = 1e-06
OUT_SCALE = 0.8


def cut_along(x, dim, peers):
    before, after = (x.shape[:dim], x.shape[dim + 1 :])
    return jnp.moveaxis(x.reshape(*before, peers, -1, *after), dim, 0)


def sum_at_owner(x, axis, dim):
    peers = lax.axis_size(axis)
    tiles = lax.all_to_all(cut_along(x, dim, peers), axis, 0, 0, tiled=True)
    return jnp.sum(tiles.astype(jnp.float32), axis=0)


def update_map(carried, queries, keys, vals, allowed):
    row_max, totals, accum = carried
    scores = jnp.einsum(
        "qgrd,kgd->grqk", queries, keys, preferred_element_type=jnp.float32
    ) * HEAD_DIM ** (-0.5)
    scores = jnp.where(allowed[None, None], scores, -jnp.inf)
    new_max = jnp.maximum(row_max, jnp.max(scores, axis=-1))
    safe_max = jnp.where(new_max == -jnp.inf, 0.0, new_max)
    exp_terms = jnp.exp(scores - safe_max[..., None])
    rescale = jnp.exp(row_max - safe_max)
    totals = totals * rescale + jnp.sum(exp_terms, axis=-1)
    accum = accum * rescale[..., None] + jnp.einsum(
        "grqk,kgv->grqv", exp_terms.astype(jnp.bfloat16), vals, preferred_element_type=jnp.float32
    )
    return (new_max, totals, accum)


def fold_piece(carried, piece, q_first, q_second, query_pos, shape_info):
    kv_here, head_dim, val_dim = shape_info
    piece_rows = piece.shape[0]
    key_block = math.gcd(piece_rows, 1024)
    num_blocks = piece_rows // key_block
    last_query = jnp.max(query_pos)

    def advance(block_no, carry_now):
        first_key = block_no * key_block

        def compute(carry_in):
            rows_now = lax.dynamic_slice_in_dim(piece, block_no * key_block, key_block, 0)
            key_first = rows_now[:, : kv_here * head_dim].reshape(key_block, kv_here, head_dim)
            key_second = rows_now[:, kv_here * head_dim : 2 * kv_here * head_dim].reshape(
                key_block, kv_here, head_dim
            )
            vals = rows_now[:, 2 * kv_here * head_dim :].reshape(key_block, kv_here, val_dim)
            key_pos = first_key + lax.iota(jnp.int32, key_block)
            allowed = (key_pos[None, :] <= query_pos[:, None]) & (key_pos[None, :] >= 0)
            first_map = update_map(carry_in[0:3], q_first, key_first, vals, allowed)
            second_map = update_map(carry_in[3:6], q_second, key_second, vals, allowed)
            return first_map + second_map

        def unchanged(carry_in):
            return carry_in

        return lax.cond(first_key > last_query, unchanged, compute, carry_now)

    return lax.fori_loop(0, num_blocks, advance, carried)


def shards(
    stream_in,
    queries_one,
    queries_two,
    keys_one,
    keys_two,
    values,
    lambdas,
    head_gain,
    out_weight,
    norm_gain,
    expert_ids,
    route_weight,
    gate_weight,
    up_weight,
    down_weight,
):
    rows_q = queries_one.shape[0]
    heads_here = queries_one.shape[1] // HEAD_DIM
    kv_here = keys_one.shape[1] // HEAD_DIM
    per_kv = heads_here // kv_here
    position = lax.axis_index("sp")
    query_pos = position * rows_q + lax.iota(jnp.int32, rows_q)
    q_first = queries_one.reshape(rows_q, kv_here, per_kv, HEAD_DIM)
    q_second = queries_two.reshape(rows_q, kv_here, per_kv, HEAD_DIM)
    packed = jnp.concatenate([keys_one, keys_two, values], 1)
    shape_info = (kv_here, HEAD_DIM, VAL_DIM)
    max_init = jnp.full((kv_here, per_kv, rows_q), -jnp.inf, jnp.float32)
    sum_init = jnp.zeros((kv_here, per_kv, rows_q), jnp.float32)
    acc_init = jnp.zeros((kv_here, per_kv, rows_q, VAL_DIM), jnp.float32)
    initial = (max_init, sum_init, acc_init, max_init, sum_init, acc_init)
    final = fold_piece(
        initial,
        lax.all_gather(packed, "sp", axis=0, tiled=True),
        q_first,
        q_second,
        query_pos,
        shape_info,
    )
    mix_first = final[2] / final[1][..., None]
    mix_second = final[5] / final[4][..., None]
    difference = mix_first - lambdas.reshape(kv_here, per_kv, 1, 1) * mix_second
    mean_sq = jnp.mean(difference * difference, axis=-1, keepdims=True)
    normed_heads = (difference * lax.rsqrt(mean_sq + EPS) * head_gain * OUT_SCALE).astype(
        jnp.bfloat16
    )
    heads_out = normed_heads.transpose(2, 0, 1, 3).reshape(rows_q, heads_here * VAL_DIM)
    rows_here = stream_in.shape[0]
    picked_rows = heads_out
    attended = sum_at_owner(
        jnp.dot(picked_rows, out_weight, preferred_element_type=jnp.float32).astype(jnp.bfloat16),
        "tp",
        0,
    )
    stream = stream_in.astype(jnp.float32) + attended
    normed = (
        stream * lax.rsqrt(jnp.mean(stream * stream, axis=-1, keepdims=True) + EPS) * norm_gain
    ).astype(jnp.bfloat16)
    top_count = expert_ids.shape[1]
    experts_all = lax.axis_size("sp")
    slot_cap = 2 * top_count * rows_here // experts_all
    flat_ids = expert_ids.reshape(-1)
    one_hot = (flat_ids[:, None] == lax.iota(jnp.int32, experts_all)[None, :]).astype(jnp.int32)
    ranks = jnp.sum((jnp.cumsum(one_hot, axis=0) - 1) * one_hot, axis=1)
    slots = flat_ids * slot_cap + ranks
    selector = (slots[None, :] == lax.iota(jnp.int32, experts_all * slot_cap)[:, None]).astype(
        jnp.bfloat16
    )
    selector = jnp.sum(selector.reshape(experts_all * slot_cap, rows_here, top_count), axis=2)
    send_rows = jnp.dot(selector, normed, preferred_element_type=jnp.float32).astype(jnp.bfloat16)
    received = lax.all_to_all(send_rows, "sp", split_axis=0, concat_axis=0, tiled=True)
    all_rows = lax.all_gather(received, "tp", axis=0, tiled=True)
    picked_rows = all_rows
    gate = jnp.dot(picked_rows, gate_weight[0], preferred_element_type=jnp.float32)
    upper = jnp.dot(picked_rows, up_weight[0], preferred_element_type=jnp.float32)
    hidden = (jax.nn.silu(gate) * upper).astype(jnp.bfloat16)
    summed = lax.psum_scatter(
        jnp.dot(hidden, down_weight[0], preferred_element_type=jnp.float32).astype(jnp.bfloat16),
        "tp",
        scatter_dimension=0,
        tiled=True,
    )
    returned = lax.all_to_all(summed, "sp", split_axis=0, concat_axis=0, tiled=True)
    picked = jnp.take(returned, slots, axis=0).reshape(rows_here, top_count, -1).astype(jnp.float32)
    routed = jnp.sum(picked * route_weight[:, :, None], axis=1)
    return (stream + routed).astype(jnp.bfloat16)


def solution(mesh):
    return jax.shard_map(
        shards,
        mesh=mesh,
        in_specs=(
            P(("sp", "tp"), None),
            P("sp", "tp"),
            P("sp", "tp"),
            P("sp", "tp"),
            P("sp", "tp"),
            P("sp", "tp"),
            P("tp"),
            P(),
            P("tp", None),
            P(),
            P(("sp", "tp"), None),
            P(("sp", "tp"), None),
            P("sp", None, "tp"),
            P("sp", None, "tp"),
            P("sp", "tp", None),
        ),
        out_specs=P(("sp", "tp"), None),
        check_vma=False,
    )
```

profile of v0, /device:TPU:7, one launch (start us, length us, event | category | flops | bytes accessed | tf_op | source)
XLA Modules:
  0.0 465.1 jit_solution(7342264499680508700)
XLA Ops:
  6.5 1.8 pad_maximum_fusion
  11.4 101.4 %all-gather.3.cloned.1.call-done = bf16[16384,512]{1,0:T(8,128)(2,1)} async-done(((bf16[256,512]{1,0:T(8,128)(2,1)}), bf16[16384,512]{1,0:T(8,128)(2,1)}) %all-gather.3.cloned.1.call-update) | async-done | bytes 16777232 | tf_op jit(solution)/shard_map/all_gather | solution.py:108
  112.8 19.9 %while.24 = (s32[]{:T(128)}, f32[1,2,256]{2,1,0:T(2,128)S(1)}, f32[1,2,256]{2,1,0:T(2,128)S(1)}, f32[1,2,256,256]{3,2,1,0:T(8,128)S(1)}, f32[1,2,256]{2,1,0:T(2,...) while((s32[]{:T(128)}, f32[1,2,256]{2,1,0:T(2,128)S(1)}, ...), condition=%wide.region_8.9_spmd.clone, body=%wide.region_1.8_spmd.clone.sunk | while | flops 813707520 | bytes 17390044 | solution.py:72
  113.5 7.3 %conditional.3 = (f32[1,2,256]{2,1,0:T(2,128)S(1)}, f32[1,2,256]{2,1,0:T(2,128)S(1)}, f32[1,2,256,256]{3,2,1,0:T(8,128)S(1)}, f32[1,2,256]{2,1,0:T(2,128)S(1)}, ...) conditional(s32[]{:T(128)} %convert_element_type.98, (s32[]{:T(128)}, s32[]{:T(128)}, s32[]{:T(128)}, ...), branch_computations={%region_2.6_spmd, %region_7.7_spmd} | conditional | flops 813707520 | bytes 17380510 | solution.py:70
  113.9 1.4 fusion.43
  115.7 1.7 fusion.7
  117.4 1.4 fusion.42
  118.8 1.7 fusion.6
  135.3 1.7 convolution_convert_fusion.1
  137.0 4.4 all-to-all-start
  142.4 11.8 %all-to-all-done = bf16[4,64,2048]{2,1,0:T(8,128)(2,1)S(1)} async-done(((bf16[4,64,2048]{2,1,0:T(8,128)(2,1)}), bf16[4,64,2048]{2,1,0:T(8,128)(2,1)S(1)}, u32[]{:S(2)}, u32[]{:S(2)}) %all-to-all-start) | async-done | bytes 1048608 | tf_op jit(solution)/shard_map/all_to_all | solution.py:23
  155.7 1.2 all_to_all.20
  157.0 142.1 %all_to_all.29 = bf16[64,4,2048]{2,1,0:T(4,128)(2,1)S(1)} all-to-all(bf16[64,4,2048]{2,1,0:T(4,128)(2,1)} %all_to_all.20), channel_id=1, replica_groups=mesh['sp'=64,'tp'=4] {'sp'}, dimensions={0} | all-to-all | bytes 2097152 | tf_op jit(solution)/shard_map/all_to_all | solution.py:145
  300.5 45.2 %all-gather.5.cloned.1.call-done = bf16[1024,2048]{1,0:T(8,128)(2,1)} async-done(((bf16[256,2048]{1,0:T(8,128)(2,1)}), bf16[1024,2048]{1,0:T(8,128)(2,1)}) %all-gather.5.cloned.1.call-update) | async-done | bytes 4194320 | tf_op jit(solution)/shard_map/all_gather | solution.py:146
  345.7 4.8 %fusion.25 = f32[1024,256]{1,0:T(8,128)} fusion(bf16[1024,2048]{1,0:T(8,128)(2,1)} %all-gather.5.cloned.1.call-done, bf16[1,2048,256]{2,1,0:T(8,128)(2,1)} %param.31), kind=kOutput, calls=%fused_computation.48 | convolution fusion | flops 1073741824 | bytes 6291456 | tf_op jit(solution)/shard_map/dot_general | solution.py:148
  350.5 9.1 %convolution_convert_fusion = bf16[1024,2048]{1,0:T(8,128)(2,1)} fusion(bf16[1024,2048]{1,0:T(8,128)(2,1)} %all-gather.5.cloned.1.call-done, bf16[1,256,2048]{2,1,0:T(8,128)(2,1)S(1)} %copy-done.9, bf16[1,2048,256]{2,1,0:T(8,128)(2,1)} %param.32, f32[1024,256]{1,0:T(8,128)} %fusion.25), kind=kOutput, calls=%fused_computation.40 | convolution fusion | flops 2151153664 | bytes 11534336 | tf_op jit(solution)/shard_map/dot_general | solution.py:152
  359.6 50.0 %reduce-scatter.2.cloned.1.call-done = bf16[256,2048]{1,0:T(8,128)(2,1)} async-done(((bf16[1024,2048]{1,0:T(8,128)(2,1)}), bf16[256,2048]{1,0:T(8,128)(2,1)}) %reduce-scatter.2.cloned.1.call-update) | async-done | bytes 1048592 | tf_op jit(solution)/shard_map/reduce_scatter | solution.py:151
  409.6 2.3 all_to_all.23
  411.9 11.0 %all-to-all-start.2 = ((bf16[64,4,2048]{2,1,0:T(4,128)(2,1)}), bf16[64,4,2048]{2,1,0:T(4,128)(2,1)}, u32[]{:S(2)}, u32[]{:S(2)}) async-start(bf16[64,4,2048]{2,1,0:T(4,128)(2,1)} %all_to_all.23), calls=%async_computation.3 | async-start | bytes 2097152 | tf_op jit(solution)/shard_map/all_to_all | solution.py:157
  423.3 27.6 %all-to-all-done.2 = bf16[64,4,2048]{2,1,0:T(4,128)(2,1)} async-done(((bf16[64,4,2048]{2,1,0:T(4,128)(2,1)}), bf16[64,4,2048]{2,1,0:T(4,128)(2,1)}, u32[]{:S(2)}, u32[]{:S(2)}) %all-to-all-start.2) | async-done | bytes 1048608 | tf_op jit(solution)/shard_map/all_to_all | solution.py:157
  450.9 1.3 all_to_all.25
  452.3 1.7 gather_fusion
  454.0 1.4 gather.7
  455.4 2.3 multiply_reduce_fusion
  (168 shorter events, 12.5 us)
Async XLA Ops:
  6.5 128.8 %copy-start = (bf16[512,2048]{1,0:T(8,128)(2,1)S(1)}, bf16[512,2048]{1,0:T(8,128)(2,1)}, u32[]{:S(2)}) copy-start(bf16[512,2048]{1,0:T(8,128)(2,1)} %param.27) | copy-start | bytes 6291460
  6.5 106.2 %all-gather.3.cloned.1.call-start = ((), (), s32[]{:S(2)}) async-start(), calls=%async_computation.4 | async-start | bytes 17039360 | tf_op jit(solution)/shard_map/all_gather | solution.py:108
  132.7 1.2 copy-start.8
  132.7 2.4 copy-start.6
  135.3 6.1 %copy-start.4 = (s32[64,2]{0,1:T(2,128)S(1)}, s32[64,2]{0,1:T(2,128)}, u32[]{:S(2)}) copy-start(s32[64,2]{0,1:T(2,128)} %param.29) | copy-start | bytes 1540
  137.0 17.4 %copy-start.3 = (bf16[64,2048]{1,0:T(8,128)(2,1)S(1)}, bf16[64,2048]{1,0:T(8,128)(2,1)}, u32[]{:S(2)}) copy-start(bf16[64,2048]{1,0:T(8,128)(2,1)} %param.19) | copy-start | bytes 786436
  137.0 18.2 %copy-start.5 = (f32[2048]{0:T(1024)S(1)}, f32[2048]{0:T(1024)}, u32[]{:S(2)}) copy-start(f32[2048]{0:T(1024)} %param.28) | copy-start | bytes 24580
  137.0 17.2 %all-to-all-start = ((bf16[4,64,2048]{2,1,0:T(8,128)(2,1)}), bf16[4,64,2048]{2,1,0:T(8,128)(2,1)S(1)}, u32[]{:S(2)}, u32[]{:S(2)}) async-start(bf16[4,64,2048]{2,1,0:T(8,128)(2,1)} %bitcast.93), calls=%async_computation | async-start | bytes 2097152 | tf_op jit(solution)/shard_map/all_to_all | solution.py:23
  141.4 204.3 %all-gather.5.cloned.1.call-start = ((), (), s32[]{:S(2)}) async-start(), calls=%async_computation.5 | async-start | bytes 5242880 | tf_op jit(solution)/shard_map/all_gather | solution.py:146
  154.4 0.8 copy-start.1
  300.2 50.3 %copy-start.9 = (bf16[1,256,2048]{2,1,0:T(8,128)(2,1)S(1)}, bf16[1,256,2048]{2,1,0:T(8,128)(2,1)}, u32[]{:S(2)}) copy-start(bf16[1,256,2048]{2,1,0:T(8,128)(2,1)} %param.33) | copy-start | bytes 3145732
  300.2 109.4 %reduce-scatter.2.cloned.1.call-start = ((), (), s32[]{:S(2)}) async-start(), calls=%async_computation.6 | async-start | bytes 5242880 | tf_op jit(solution)/shard_map/reduce_scatter | solution.py:151
  359.6 63.5 %copy-start.7 = (f32[64,2]{0,1:T(2,128)S(1)}, f32[64,2]{0,1:T(2,128)}, u32[]{:S(2)}) copy-start(f32[64,2]{0,1:T(2,128)} %param.30) | copy-start | bytes 1540
  411.9 39.0 %all-to-all-start.2 = ((bf16[64,4,2048]{2,1,0:T(4,128)(2,1)}), bf16[64,4,2048]{2,1,0:T(4,128)(2,1)}, u32[]{:S(2)}, u32[]{:S(2)}) async-start(bf16[64,4,2048]{2,1,0:T(4,128)(2,1)} %all_to_all.23), calls=%async_computation.3 | async-start | bytes 2097152 | tf_op jit(solution)/shard_map/all_to_all | solution.py:157
  454.0 3.8 copy-start.2
Sparse Core Ops, SparseCore 0:
  10.1 102.5 all-gather.2
  300.4 45.2 all-gather.4
  359.8 49.8 reduce-scatter.1
where the time goes:
time: 471 us; the launch traced here: 465 us
  waiting for transfers between devices  236 us (50%)
  blocking collectives  142 us (30%)
  matrix products  22.3 us (5%)
  starting transfers between devices  15.5 us (3%)
  local copies, waits for them, and re-layouts  14.3 us (3%)
  between operations  13.4 us (3%)
  loops' own time  12.5 us (3%)
  other arithmetic  8.84 us (2%)
    all_to_all x1, blocking collectives, shards(): lax.all_to_all(send_rows, 'sp', split_axis=0, concat_axis=0, tiled=True)  142 us
    all_gather x1, waiting for transfers between devices, shards(): lax.all_gather(packed, 'sp', axis=0, tiled=True)  101 us
    reduce_scatter x1, waiting for transfers between devices, shards(): lax.psum_scatter(jnp.dot(hidden, down_weight[0], preferred_element_type=j...  50 us
    all_gather x1, waiting for transfers between devices, shards(): all_rows = lax.all_gather(received, 'tp', axis=0, tiled=True)  45.2 us
    all_to_all x1, waiting for transfers between devices, shards(): lax.all_to_all(summed, 'sp', split_axis=0, concat_axis=0, tiled=True)  27.6 us
    all_to_all x1, waiting for transfers between devices, sum_at_owner(): tiles = lax.all_to_all(cut_along(x, dim, peers), axis, 0, 0, tiled=True)  11.8 us
    another operation x1, loops' own time, fold_piece(): return lax.fori_loop(0, num_blocks, advance, carried)  11.8 us
    all_to_all x1, starting transfers between devices, shards(): lax.all_to_all(summed, 'sp', split_axis=0, concat_axis=0, tiled=True)  11 us
  transfers between devices with their start and end apart: 5, of which 5 were waited for; matrix products, arithmetic and copies ran while one was open for 1% of the time, Pallas kernels for 0%

commit v1 on v0

v1 whole, which is shorter than its diff:
```python
import functools
import math

import jax
import jax.numpy as jnp
from jax import lax
from jax.experimental import pallas as pl
from jax.experimental.pallas import tpu as pltpu
from jax.sharding import PartitionSpec as P

HEAD_DIM = 128
VAL_DIM = 256
EPS = 1e-06
OUT_SCALE = 0.8
SCALE2 = HEAD_DIM ** (-0.5) * math.log2(math.e)
BK = 1024


def flash_kernel(n_sp, q_ref, kv_ref, lam_ref, gain_ref, out_ref, m_ref, l_ref, acc_ref):
    me = lax.axis_index("sp")
    rows = q_ref.shape[2]
    half = rows // 2

    def update(run, block, masked, first_row):
        start = pl.multiple_of(block * BK, BK)
        v = kv_ref[pl.ds(start, BK), 2 * HEAD_DIM :]
        if masked:
            row = first_row + lax.rem(lax.broadcasted_iota(jnp.int32, (rows, BK), 0), half)
            keep = start + lax.broadcasted_iota(jnp.int32, (rows, BK), 1) <= row
        for k in range(2):
            q = q_ref[run, k]
            keys = kv_ref[pl.ds(start, BK), k * HEAD_DIM : (k + 1) * HEAD_DIM]
            s = lax.dot_general(q, keys, (((1,), (1,)), ((), ())), preferred_element_type=jnp.float32)
            if masked:
                s = jnp.where(keep, s, -jnp.inf)
            old = m_ref[k]
            new = jnp.maximum(old, jnp.max(s, axis=1, keepdims=True))
            terms = jnp.exp2((s - new[:, :1]) * SCALE2)
            fade = jnp.exp2((old - new) * SCALE2)
            part = terms[:, :128]
            for c in range(1, BK // 128):
                part = part + terms[:, c * 128 : (c + 1) * 128]
            m_ref[k] = new
            l_ref[k] = l_ref[k] * fade + part
            acc_ref[k] = acc_ref[k] * fade[:, :1] + jnp.dot(
                terms.astype(jnp.bfloat16), v, preferred_element_type=jnp.float32
            )

    for run in range(2):
        first_row = me * 2 * half if run == 0 else (n_sp - 1 - me) * 2 * half + half
        m_ref[...] = jnp.full(m_ref.shape, -1e30, jnp.float32)
        l_ref[...] = jnp.zeros(l_ref.shape, jnp.float32)
        acc_ref[...] = jnp.zeros(acc_ref.shape, jnp.float32)
        full = first_row // BK
        lax.fori_loop(0, full, lambda i, c: (update(run, i, False, first_row), c)[1], 0)
        update(run, full, True, first_row)
        mix = [acc_ref[k] / jnp.sum(l_ref[k], axis=1, keepdims=True) for k in range(2)]
        for h in range(2):
            piece = slice(h * half, (h + 1) * half)
            diff = mix[0][piece] - lam_ref[h] * mix[1][piece]
            ms = jnp.mean(diff * diff, axis=1, keepdims=True)
            res = diff * lax.rsqrt(ms + EPS) * gain_ref[...] * OUT_SCALE
            out_ref[run * half : (run + 1) * half, h * VAL_DIM : (h + 1) * VAL_DIM] = res.astype(jnp.bfloat16)


def flash(q, kv, lambdas, gain, n_sp):
    rows = q.shape[2]
    return pl.pallas_call(
        functools.partial(flash_kernel, n_sp),
        out_shape=jax.ShapeDtypeStruct((rows, 2 * VAL_DIM), jnp.bfloat16),
        in_specs=[
            pl.BlockSpec(memory_space=pltpu.VMEM),
            pl.BlockSpec(memory_space=pltpu.VMEM),
            pl.BlockSpec(memory_space=pltpu.SMEM),
            pl.BlockSpec(memory_space=pltpu.VMEM),
        ],
        out_specs=pl.BlockSpec(memory_space=pltpu.VMEM),
        scratch_shapes=[
            pltpu.VMEM((2, rows, 128), jnp.float32),
            pltpu.VMEM((2, rows, 128), jnp.float32),
            pltpu.VMEM((2, rows, VAL_DIM), jnp.float32),
        ],
        compiler_params=pltpu.CompilerParams(vmem_limit_bytes=48 * 1024 * 1024),
        name="flash",
    )(q, kv, lambdas, gain)


def shards(
    stream_in, queries_one, queries_two, keys_one, keys_two, values, lambdas, head_gain, out_weight,
    norm_gain, expert_ids, route_weight, gate_weight, up_weight, down_weight,
):
    n_sp, n_tp = lax.axis_size("sp"), lax.axis_size("tp")
    rows = queries_one.shape[0]
    half = rows // 2
    feats = stream_in.shape[1] // n_tp
    bf, f32 = jnp.bfloat16, jnp.float32

    mirror = [(s, n_sp - 1 - s) for s in range(n_sp)]
    home = [
        (s * n_tp + t, (s if t < n_tp // 2 else n_sp - 1 - s) * n_tp + t)
        for s in range(n_sp)
        for t in range(n_tp)
    ]
    q_pair = jnp.stack([queries_one, queries_two])
    q_far = lax.ppermute(q_pair[:, half:], "sp", mirror)
    q_all = jnp.stack([q_pair[:, :half], q_far])
    q_all = q_all.reshape(2, 2, half, 2, HEAD_DIM).transpose(0, 1, 3, 2, 4).reshape(2, 2, rows, HEAD_DIM)
    stream_far = lax.ppermute(stream_in, ("sp", "tp"), home)
    stream_mine = lax.all_to_all(stream_far, "tp", 1, 0, tiled=True).astype(f32)
    ids = lax.all_gather(lax.ppermute(expert_ids, ("sp", "tp"), home), "tp", axis=0, tiled=True)
    route = lax.all_gather(lax.ppermute(route_weight, ("sp", "tp"), home), "tp", axis=0, tiled=True)
    out_cols = lax.all_to_all(out_weight, "tp", 1, 0, tiled=True)
    down_cols = lax.all_to_all(down_weight[0], "tp", 1, 0, tiled=True)
    gain_mine = lax.dynamic_slice_in_dim(norm_gain, lax.axis_index("tp") * feats, feats, 0)

    cap = 16
    flat = ids.reshape(-1)
    one_hot = (flat[:, None] == lax.iota(jnp.int32, n_sp)[None, :]).astype(bf)
    lower = (lax.iota(jnp.int32, 2 * rows)[:, None] > lax.iota(jnp.int32, 2 * rows)[None, :]).astype(bf)
    before = jnp.dot(lower, one_hot, preferred_element_type=f32)
    ranks = jnp.sum(before * one_hot.astype(f32), axis=1).astype(jnp.int32)
    slots = (flat * cap + ranks).reshape(rows, 2)
    pick = [(slots[:, k][:, None] == lax.iota(jnp.int32, n_sp * cap)[None, :]).astype(bf) for k in range(2)]

    packed = jnp.concatenate([keys_one, keys_two, values], 1)
    kv = lax.all_gather(packed, "sp", axis=0, tiled=True)
    heads = flash(q_all, kv, lambdas, head_gain[None], n_sp)
    heads_all = lax.all_gather(heads, "tp", axis=1, tiled=True)
    stream = stream_mine + jnp.dot(heads_all, out_cols, preferred_element_type=f32)
    ssq = lax.psum(jnp.sum(stream * stream, axis=1), "tp")
    inv = lax.rsqrt(ssq / (feats * n_tp) + EPS)
    normed = (stream * inv[:, None] * gain_mine).astype(bf)
    send = lax.dot_general(
        pick[0] + pick[1], normed, (((0,), (0,)), ((), ())), preferred_element_type=f32
    ).astype(bf)
    got = lax.all_to_all(send, "sp", 0, 0, tiled=True)
    got = lax.all_gather(got, "tp", axis=1, tiled=True)
    gate = jnp.dot(got, gate_weight[0], preferred_element_type=f32)
    upper = jnp.dot(got, up_weight[0], preferred_element_type=f32)
    hidden = (jax.nn.silu(gate) * upper).astype(bf)
    hidden = lax.all_gather(hidden, "tp", axis=1, tiled=True)
    result = jnp.dot(hidden, down_cols, preferred_element_type=f32).astype(bf)
    back = lax.all_to_all(result, "sp", 0, 0, tiled=True)
    for k in range(2):
        stream = stream + route[:, k][:, None] * jnp.dot(pick[k], back, preferred_element_type=f32)
    mixed = lax.all_to_all(stream.astype(bf), "tp", 0, 1, tiled=True)
    return lax.ppermute(mixed, ("sp", "tp"), home)


def solution(mesh):
    return jax.shard_map(
        shards,
        mesh=mesh,
        in_specs=(
            P(("sp", "tp"), None),
            P("sp", "tp"),
            P("sp", "tp"),
            P("sp", "tp"),
            P("sp", "tp"),
            P("sp", "tp"),
            P("tp"),
            P(),
            P("tp", None),
            P(),
            P(("sp", "tp"), None),
            P(("sp", "tp"), None),
            P("sp", None, "tp"),
            P("sp", None, "tp"),
            P("sp", "tp", None),
        ),
        out_specs=P(("sp", "tp"), None),
        check_vma=False,
    )
```

time: 471 us -> 393 us (0.83)
  blocking collectives: 142 us -> 85.3 us
  waiting for transfers between devices: 236 us -> 184 us
  starting transfers between devices: 15.5 us -> 47.1 us
  Pallas kernels: 0 us -> 28.9 us
  loops' own time: 12.5 us -> 0 us
  matrix products: 22.3 us -> 15.3 us
    all_to_all x1 -> x3, blocking collectives: 142 us -> 66.8 us  [the longest x1 40.6 us: shards(): got = lax.all_to_all(send, 'sp', 0, 0, tiled=True)]
    ppermute x0 -> x5, waiting for transfers between devices: none -> 53.8 us  [the longest x1 19.4 us: shards(): lax.ppermute(route_weight, ('sp', 'tp'), home)]
    reduce_scatter x1 -> x0, waiting for transfers between devices: 50 us -> none  [shards(): lax.psum_scatter(jnp.dot(hidden, down_weight[0], preferred_element_type=j...]
    all_to_all x2 -> x3, waiting for transfers between devices: 39.4 us -> 0.43 us  [the longest x1 0.43 us: shards(): stream_mine = lax.all_to_all(stream_far, 'tp', 1, 0, tiled=True).astype(f32)]
    pallas_call x0 -> x1, Pallas kernels: none -> 28.9 us  [flash(): pl.pallas_call(functools.partial(flash_kernel, n_sp), out_shape=jax.Shape...]
    ppermute x0 -> x5, starting transfers between devices: none -> 25.3 us  [the longest x1 10.5 us: shards(): stream_far = lax.ppermute(stream_in, ('sp', 'tp'), home)]
    all_gather x2 -> x4, waiting for transfers between devices: 147 us -> 130 us  [the longest x1 62.7 us: shards(): kv = lax.all_gather(packed, 'sp', axis=0, tiled=True)]
    another operation x17 -> x0, loops' own time: 12.5 us -> none  [the longest x1 11.8 us: fold_piece(): return lax.fori_loop(0, num_blocks, advance, carried)]
  transfers between devices with their start and end apart: 5 -> 12, of which waited for: 5 -> 8; matrix products, arithmetic and copies ran while one was open for 1% -> 3% of each run, Pallas kernels for 0% -> 7%
where the time goes in v1:
time: 393 us; the launch traced here: 391 us
  waiting for transfers between devices  184 us (47%)
  blocking collectives  85.3 us (22%)
  starting transfers between devices  47.1 us (12%)
  Pallas kernels  28.9 us (7%)
  matrix products  15.3 us (4%)
  between operations  13.4 us (3%)
  local copies, waits for them, and re-layouts  11.6 us (3%)
  other arithmetic  5.3 us (1%)
    all_gather x1, waiting for transfers between devices, shards(): kv = lax.all_gather(packed, 'sp', axis=0, tiled=True)  62.7 us
    all_gather x1, waiting for transfers between devices, shards(): got = lax.all_gather(got, 'tp', axis=1, tiled=True)  45.6 us
    all_to_all x1, blocking collectives, shards(): got = lax.all_to_all(send, 'sp', 0, 0, tiled=True)  40.6 us
    pallas_call x1, Pallas kernels, flash(): pl.pallas_call(functools.partial(flash_kernel, n_sp), out_shape=jax.Shape...  28.9 us
    all_gather x1, waiting for transfers between devices, shards(): hidden = lax.all_gather(hidden, 'tp', axis=1, tiled=True)  21.2 us
    ppermute x1, waiting for transfers between devices, shards(): lax.ppermute(route_weight, ('sp', 'tp'), home)  19.4 us
    all_to_all x1, blocking collectives, shards(): down_cols = lax.all_to_all(down_weight[0], 'tp', 1, 0, tiled=True)  17.2 us
    ppermute x1, waiting for transfers between devices, shards(): stream_far = lax.ppermute(stream_in, ('sp', 'tp'), home)  16.3 us
  transfers between devices with their start and end apart: 12, of which 8 were waited for; matrix products, arithmetic and copies ran while one was open for 3% of the time, Pallas kernels for 7%

profile of v1, /device:TPU:7, one launch (start us, length us, event | category | flops | bytes accessed | tf_op | source)
XLA Modules:
  0.0 390.6 jit_solution(3796240094126680283)
XLA Ops:
  8.4 10.5 %collective-permute-start = (bf16[64,2048]{1,0:T(8,128)(2,1)}, bf16[64,2048]{1,0:T(8,128)(2,1)S(1)}, u32[]{:S(2)}, u32[]{:S(2)}) collective-permute-start(bf16[64,2048]{1,0:T(8,128)(2,1)} %param.15), channel_id=1, source_target_pairs={{0,0},{1,1},{2,254},{3,255},{4,4},{5,5},{6,250},{7,251},{8,8},{9,9... | collective-permute-start | bytes 786440 | tf_op jit(solution)/shard_map/ppermute | solution.py:108
  20.5 16.3 %collective-permute-done = bf16[64,2048]{1,0:T(8,128)(2,1)S(1)} collective-permute-done((bf16[64,2048]{1,0:T(8,128)(2,1)}, bf16[64,2048]{1,0:T(8,128)(2,1)S(1)}, u32[]{:S(2)}, u32[]{:S(2)}) %collective-permute-start) | collective-permute-done | bytes 262176 | tf_op jit(solution)/shard_map/ppermute | solution.py:108
  37.5 4.1 %all-to-all-start = ((bf16[64,4,512]{2,0,1:T(8,128)(2,1)}), bf16[64,4,512]{2,0,1:T(8,128)(2,1)}, u32[]{:S(2)}, u32[]{:S(2)}) async-start(bf16[64,4,512]{2,0,1:T(8,128)(2,1)} %bitcast.50), calls=%async_computation | async-start | bytes 524288 | tf_op jit(solution)/shard_map/all_to_all | solution.py:109
  45.7 5.5 %all-to-all-start.1 = ((bf16[512,4,512]{0,2,1:T(8,128)(2,1)}), bf16[512,4,512]{0,2,1:T(8,128)(2,1)S(1)}, u32[]{:S(2)}, u32[]{:S(2)}) async-start(bf16[512,4,512]{0,2,1:T(8,128)(2,1)} %bitcast.7), calls=%async_computation.1 | async-start | bytes 4194304 | tf_op jit(solution)/shard_map/all_to_all | solution.py:112
  51.2 62.7 %all-gather.7.cloned.1.call-done.kv_ref = bf16[16384,512]{1,0:T(8,128)(2,1)} async-done(((bf16[256,512]{1,0:T(8,128)(2,1)}), bf16[16384,512]{1,0:T(8,128)(2,1)}) %all-gather.7.cloned.1.call-update) | async-done | bytes 16777232 | tf_op jit(solution)/shard_map/all_gather | solution.py:126
  113.8 28.9 %flash.1 = bf16[256,512]{1,0:T(8,128)(2,1)} custom-call(bf16[2,2,256,128]{3,2,1,0:T(8,128)(2,1)S(1)} %bitcast.51, bf16[16384,512]{1,0:T(8,128)(2,1)} %all-gather.7.cloned.1.call-done.kv_ref, f32[2]{0:T(128)S(1)} %copy-done.2, f32[1,256]{1,0:T(1,128)S(1)} %bitcast.52), custom_call_target="tpu_custom_call" | custom-call | tf_op jit(solution)/shard_map/flash/pallas_call | solution.py:68
  142.8 3.4 collective-permute-start.3
  147.0 4.0 %collective-permute-done.3 = s32[64,2]{0,1:T(2,128)S(1)} collective-permute-done((s32[64,2]{0,1:T(2,128)S(1)}, s32[64,2]{0,1:T(2,128)S(1)}, u32[]{:S(2)}, u32[]{:S(2)}) %collective-permute-start.3) | collective-permute-done | bytes 544 | tf_op jit(solution)/shard_map/ppermute | solution.py:110
  151.0 5.5 %all-gather.1 = s32[4,64,2]{1,2,0:T(2,128)S(1)} all-gather(s32[1,64,2]{1,2,0:T(2,128)S(1)} %bitcast.73), channel_id=1, replica_groups=mesh['sp'=64,'tp'=4] {'tp'}, dimensions={0}, use_global_device_ids=true | all-gather | bytes 2560 | tf_op jit(solution)/shard_map/all_gather | solution.py:110
  163.4 2.9 multiply_reduce_fusion
  166.3 7.8 %psum.7 = f32[256]{0:T(256)S(1)} all-reduce(f32[256]{0:T(256)S(1)} %get-tuple-element.11), channel_id=1, replica_groups=mesh['sp'=64,'tp'=4] {'tp'}, use_global_device_ids=true, to_apply=%region_2.0 | all-reduce | flops 256 | bytes 2048 | tf_op jit(solution)/shard_map/psum | solution.py:130
  175.9 40.6 %all_to_all.94 = bf16[64,16,512]{2,1,0:T(8,128)(2,1)} all-to-all(bf16[64,16,512]{2,1,0:T(8,128)(2,1)S(1)} %bitcast.63), channel_id=1, replica_groups=mesh['sp'=64,'tp'=4] {'sp'}, dimensions={0} | all-to-all | bytes 2097152 | tf_op jit(solution)/shard_map/all_to_all | solution.py:136
  216.7 45.6 %all-gather.11.cloned.1.call-done = bf16[1024,2048]{1,0:T(8,128)(2,1)} async-done(((bf16[1024,512]{1,0:T(8,128)(2,1)}), bf16[1024,2048]{1,0:T(8,128)(2,1)}) %all-gather.11.cloned.1.call-update) | async-done | bytes 4194320 | tf_op jit(solution)/shard_map/all_gather | solution.py:137
  262.3 3.6 fusion.6
  268.6 17.2 %all_to_all.95 = bf16[256,4,512]{0,2,1:T(8,128)(2,1)S(1)} all-to-all(bf16[256,4,512]{0,2,1:T(8,128)(2,1)S(1)} %bitcast.59), channel_id=1, replica_groups=mesh['sp'=64,'tp'=4] {'tp'}, dimensions={1} | all-to-all | bytes 2097152 | tf_op jit(solution)/shard_map/all_to_all | solution.py:113
  286.4 21.2 %all-gather.13.cloned.1.call-done = bf16[1024,1024]{1,0:T(8,128)(2,1)} async-done(((bf16[1024,256]{1,0:T(8,128)(2,1)}), bf16[1024,1024]{1,0:T(8,128)(2,1)}) %all-gather.13.cloned.1.call-update) | async-done | bytes 2097168 | tf_op jit(solution)/shard_map/all_gather | solution.py:141
  307.6 3.8 convolution_convert_fusion
  311.5 11.9 %all-to-all-start.4 = ((bf16[64,16,512]{2,1,0:T(8,128)(2,1)}), bf16[64,16,512]{2,1,0:T(8,128)(2,1)S(1)}, u32[]{:S(2)}, u32[]{:S(2)}) async-start(bf16[64,16,512]{2,1,0:T(8,128)(2,1)} %bitcast.61), calls=%async_computation.4 | async-start | bytes 2097152 | tf_op jit(solution)/shard_map/all_to_all | solution.py:143
  323.3 7.2 %collective-permute-start.2 = (f32[64,2]{0,1:T(2,128)S(1)}, f32[64,2]{0,1:T(2,128)S(1)}, u32[]{:S(2)}, u32[]{:S(2)}) collective-permute-start(f32[64,2]{0,1:T(2,128)S(1)} %copy-done.10), channel_id=1, source_target_pairs={{0,0},{1,1},{2,254},{3,255},{4,4},{5,5},{6,250},{7,251},{8,8},{9,9... | collective-permute-start | bytes 1544 | tf_op jit(solution)/shard_map/ppermute | solution.py:111
  330.5 19.4 %collective-permute-done.2 = f32[64,2]{0,1:T(2,128)S(1)} collective-permute-done((f32[64,2]{0,1:T(2,128)S(1)}, f32[64,2]{0,1:T(2,128)S(1)}, u32[]{:S(2)}, u32[]{:S(2)}) %collective-permute-start.2) | collective-permute-done | bytes 544 | tf_op jit(solution)/shard_map/ppermute | solution.py:111
  349.9 5.1 %all-gather = f32[4,64,2]{1,2,0:T(2,128)S(1)} all-gather(f32[1,64,2]{1,2,0:T(2,128)S(1)} %bitcast.74), channel_id=1, replica_groups=mesh['sp'=64,'tp'=4] {'tp'}, dimensions={0}, use_global_device_ids=true | all-gather | bytes 2560 | tf_op jit(solution)/shard_map/all_gather | solution.py:111
  356.1 8.9 %all_to_all.96 = bf16[4,64,512]{2,1,0:T(8,128)(2,1)S(1)} all-to-all(bf16[4,64,512]{2,1,0:T(8,128)(2,1)S(1)} %bitcast.66), channel_id=1, replica_groups=mesh['sp'=64,'tp'=4] {'tp'}, dimensions={0} | all-to-all | bytes 524288 | tf_op jit(solution)/shard_map/all_to_all | solution.py:146
  365.1 4.3 %collective-permute-start.4 = (bf16[64,2048]{1,0:T(8,128)(2,1)S(1)}, bf16[64,2048]{1,0:T(8,128)(2,1)S(1)}, u32[]{:S(2)}, u32[]{:S(2)}) collective-permute-start(bf16[64,2048]{1,0:T(8,128)(2,1)S(1)} %bitcast.67), channel_id=1, source_target_pairs={{0,0},{1,1},{2,254},{3,255},{4,4},{5,5},{6,250},{7,251},{8,8},{9,9... | collective-permute-start | bytes 786440 | tf_op jit(solution)/shard_map/ppermute | solution.py:147
  369.3 14.1 %collective-permute-done.4 = bf16[64,2048]{1,0:T(8,128)(2,1)S(1)} collective-permute-done((bf16[64,2048]{1,0:T(8,128)(2,1)S(1)}, bf16[64,2048]{1,0:T(8,128)(2,1)S(1)}, u32[]{:S(2)}, u32[]{:S(2)}) %collective-permute-start.4) | collective-permute-done | bytes 262176 | tf_op jit(solution)/shard_map/ppermute | solution.py:147
  (70 shorter events, 22.8 us)
Async XLA Ops:
  6.5 255.8 %copy-start = (bf16[1,2048,256]{2,1,0:T(8,128)(2,1)S(1)}, bf16[1,2048,256]{2,1,0:T(8,128)(2,1)}, u32[]{:S(2)}) copy-start(bf16[1,2048,256]{2,1,0:T(8,128)(2,1)} %param.27) | copy-start | bytes 3145732
  6.5 35.2 %copy-start.5 = (bf16[512,2048]{1,0:T(8,128)(2,1)S(1)}, bf16[512,2048]{1,0:T(8,128)(2,1)}, u32[]{:S(2)}) copy-start(bf16[512,2048]{1,0:T(8,128)(2,1)} %param.23) | copy-start | bytes 6291460
  6.5 107.3 %all-gather.7.cloned.1.call-start = ((), (), s32[]{:S(2)}) async-start(), calls=%async_computation.6 | async-start | bytes 17039360 | tf_op jit(solution)/shard_map/all_gather | solution.py:126
  8.4 28.4 %collective-permute-start = (bf16[64,2048]{1,0:T(8,128)(2,1)}, bf16[64,2048]{1,0:T(8,128)(2,1)S(1)}, u32[]{:S(2)}, u32[]{:S(2)}) collective-permute-start(bf16[64,2048]{1,0:T(8,128)(2,1)} %param.15), channel_id=1, source_target_pairs={{0,0},{1,1},{2,254},{3,255},{4,4},{5,5},{6,250},{7,251},{8,8},{9,9... | collective-permute-start | bytes 786440 | tf_op jit(solution)/shard_map/ppermute | solution.py:108
  20.5 23.7 %collective-permute-start.1 = (bf16[2,128,256]{2,1,0:T(8,128)(2,1)}, bf16[2,128,256]{2,1,0:T(8,128)(2,1)}, u32[]{:S(2)}, u32[]{:S(2)}) collective-permute-start(bf16[2,128,256]{2,1,0:T(8,128)(2,1)} %get-tuple-element.6), channel_id=1, source_target_pairs={{0,252},{4,248},{8,244},{12,240},{16,236},{20,232},{24,228},{28,22... | collective-permute-start | bytes 393224 | tf_op jit(solution)/shard_map/ppermute | solution.py:105
  37.5 8.2 %all-to-all-start = ((bf16[64,4,512]{2,0,1:T(8,128)(2,1)}), bf16[64,4,512]{2,0,1:T(8,128)(2,1)}, u32[]{:S(2)}, u32[]{:S(2)}) async-start(bf16[64,4,512]{2,0,1:T(8,128)(2,1)} %bitcast.50), calls=%async_computation | async-start | bytes 524288 | tf_op jit(solution)/shard_map/all_to_all | solution.py:109
  45.7 68.2 %copy-start.1 = (f32[256]{0:T(256)S(1)}, f32[256]{0:T(256)}, u32[]{:S(2)}) copy-start(f32[256]{0:T(256)} %param.22) | copy-start | bytes 3076
  45.7 68.2 %copy-start.2 = (f32[2]{0:T(128)S(1)}, f32[2]{0:T(128)}, u32[]{:S(2)}) copy-start(f32[2]{0:T(128)} %lam_ref.1) | copy-start | bytes 28
  45.7 113.6 %all-to-all-start.1 = ((bf16[512,4,512]{0,2,1:T(8,128)(2,1)}), bf16[512,4,512]{0,2,1:T(8,128)(2,1)S(1)}, u32[]{:S(2)}, u32[]{:S(2)}) async-start(bf16[512,4,512]{0,2,1:T(8,128)(2,1)} %bitcast.7), calls=%async_computation.1 | async-start | bytes 4194304 | tf_op jit(solution)/shard_map/all_to_all | solution.py:112
  51.2 112.3 %all-gather.9.cloned.1.call-start = ((), (), s32[]{:S(2)}) async-start(), calls=%async_computation.7 | async-start | bytes 1310720 | tf_op jit(solution)/shard_map/all_gather | solution.py:128
  113.8 29.0 %copy-start.9 = (s32[64,2]{0,1:T(2,128)S(1)}, s32[64,2]{0,1:T(2,128)}, u32[]{:S(2)}) copy-start(s32[64,2]{0,1:T(2,128)} %param.25) | copy-start | bytes 1540
  142.7 119.6 %all-gather.11.cloned.1.call-start = ((), (), s32[]{:S(2)}) async-start(), calls=%async_computation.8 | async-start | bytes 5242880 | tf_op jit(solution)/shard_map/all_gather | solution.py:137
  142.8 8.2 %collective-permute-start.3 = (s32[64,2]{0,1:T(2,128)S(1)}, s32[64,2]{0,1:T(2,128)S(1)}, u32[]{:S(2)}, u32[]{:S(2)}) collective-permute-start(s32[64,2]{0,1:T(2,128)S(1)} %copy-done.9), channel_id=1, source_target_pairs={{0,0},{1,1},{2,254},{3,255},{4,4},{5,5},{6,250},{7,251},{8,8},{9,9... | collective-permute-start | bytes 1544 | tf_op jit(solution)/shard_map/ppermute | solution.py:110
  159.3 1.3 copy-start.3
  216.5 49.4 %copy-start.8 = (bf16[1,2048,256]{2,1,0:T(8,128)(2,1)S(1)}, bf16[1,2048,256]{2,1,0:T(8,128)(2,1)}, u32[]{:S(2)}) copy-start(bf16[1,2048,256]{2,1,0:T(8,128)(2,1)} %param.28) | copy-start | bytes 3145732
  216.5 91.1 %all-gather.13.cloned.1.call-start = ((), (), s32[]{:S(2)}) async-start(), calls=%async_computation.9 | async-start | bytes 2621440 | tf_op jit(solution)/shard_map/all_gather | solution.py:141
  262.3 3.6 copy-start.7
  265.9 2.1 copy-start.6
  311.5 11.9 %copy-start.10 = (f32[64,2]{0,1:T(2,128)S(1)}, f32[64,2]{0,1:T(2,128)}, u32[]{:S(2)}) copy-start(f32[64,2]{0,1:T(2,128)} %param.26) | copy-start | bytes 1540
  311.5 43.6 %copy-start.4 = (f32[256,512]{1,0:T(8,128)S(1)}, f32[256,512]{1,0:T(8,128)}, u32[]{:S(2)}) copy-start(f32[256,512]{1,0:T(8,128)} %get-tuple-element.12) | copy-start | bytes 1572868
  311.5 43.6 %all-to-all-start.4 = ((bf16[64,16,512]{2,1,0:T(8,128)(2,1)}), bf16[64,16,512]{2,1,0:T(8,128)(2,1)S(1)}, u32[]{:S(2)}, u32[]{:S(2)}) async-start(bf16[64,16,512]{2,1,0:T(8,128)(2,1)} %bitcast.61), calls=%async_computation.4 | async-start | bytes 2097152 | tf_op jit(solution)/shard_map/all_to_all | solution.py:143
  323.3 26.6 %collective-permute-start.2 = (f32[64,2]{0,1:T(2,128)S(1)}, f32[64,2]{0,1:T(2,128)S(1)}, u32[]{:S(2)}, u32[]{:S(2)}) collective-permute-start(f32[64,2]{0,1:T(2,128)S(1)} %copy-done.10), channel_id=1, source_target_pairs={{0,0},{1,1},{2,254},{3,255},{4,4},{5,5},{6,250},{7,251},{8,8},{9,9... | collective-permute-start | bytes 1544 | tf_op jit(solution)/shard_map/ppermute | solution.py:111
  365.1 18.3 %collective-permute-start.4 = (bf16[64,2048]{1,0:T(8,128)(2,1)S(1)}, bf16[64,2048]{1,0:T(8,128)(2,1)S(1)}, u32[]{:S(2)}, u32[]{:S(2)}) collective-permute-start(bf16[64,2048]{1,0:T(8,128)(2,1)S(1)} %bitcast.67), channel_id=1, source_target_pairs={{0,0},{1,1},{2,254},{3,255},{4,4},{5,5},{6,250},{7,251},{8,8},{9,9... | collective-permute-start | bytes 786440 | tf_op jit(solution)/shard_map/ppermute | solution.py:147
Sparse Core Ops, SparseCore 0:
  10.1 103.6 all-gather.6
  142.9 20.4 all-gather.8
  216.6 45.6 all-gather.10
  268.2 39.4 all-gather.12

commit v2 on v1

--- a/solution.py
+++ b/solution.py
@@ -14,6 +14,7 @@
 OUT_SCALE = 0.8
 SCALE2 = HEAD_DIM ** (-0.5) * math.log2(math.e)
 BK = 1024
+PLANES = 8
 
 
 def flash_kernel(n_sp, q_ref, kv_ref, lam_ref, gain_ref, out_ref, m_ref, l_ref, acc_ref):
@@ -85,6 +86,326 @@
     )(q, kv, lambdas, gain)
 
 
+MESH = pl.DeviceIdType.MESH
+
+
+def post_kernel(n_sp, n_tp, group, heads, out_w, stream_in, gain, slots_row, slots_col, route, gate_h, up_h, down_h,
+                out, hall, oc, gate_w, up_w, down_w, stream, ssq, send, xbuf, hbuf, rbuf, back, mix,
+                sent, local_sem, wsem, asem, a2sem, qsem, dsem, xsem, x2sem, hsem, h2sem, bsem, fsem):
+    s, t = lax.axis_index("sp"), lax.axis_index("tp")
+    n_z = n_sp // group
+    z, w = s // group, lax.rem(s, group)
+    far_s = n_sp - 1 - s
+    cap, feats = send.shape[1], send.shape[2]
+    units = gate_w.shape[1]
+    rows = heads.shape[0]
+    half, block = rows // 2, rows // n_tp
+    f32, bf = jnp.float32, jnp.bfloat16
+
+    loads = [
+        pltpu.make_async_copy(a, b, wsem.at[i])
+        for i, (a, b) in enumerate(((out_w, oc), (gate_h, gate_w), (up_h, up_w), (down_h, down_w)))
+    ]
+    for load in loads:
+        load.start()
+
+    def side(d):
+        return lax.rem(t + d + n_tp, n_tp)
+
+    def offset(j):
+        away = (n_z // 2 - j // 2) * jnp.minimum(j, 1)
+        return away * (1 - 2 * lax.rem(j, 2))
+
+    def to_plane(j):
+        return lax.rem(z + offset(j) + n_z, n_z)
+
+    def from_plane(j):
+        return lax.rem(z - offset(j) + n_z, n_z)
+
+    def remote(src, dst, a, b, sp, tp):
+        return pltpu.make_async_remote_copy(
+            src_ref=src, dst_ref=dst, send_sem=a, recv_sem=b, device_id=(sp, tp), device_id_type=MESH)
+
+    def arrived(ref, sem):
+        remote(ref, ref, sent.at[0], sem, s, side(1)).wait_recv()
+
+    def left(ref, sem):
+        remote(ref, ref, sem, dsem.at[0], s, side(1)).wait_send()
+
+    barrier = pltpu.get_barrier_semaphore()
+
+    def hello(sp, tp):
+        pl.semaphore_signal(barrier, inc=1, device_id=(sp, tp), device_id_type=MESH)
+
+    def greet(o, c):
+        hello(lax.rem(s + o, n_sp), t)
+        return c
+
+    lax.fori_loop(1, n_sp, greet, 0)
+    for d in range(1, n_tp):
+        hello(s, side(d))
+    low = t < n_tp // 2
+
+    @pl.when(jnp.logical_not(low))
+    def _():
+        for d in range(n_tp):
+            hello(far_s, d)
+
+    pl.semaphore_wait(barrier, n_sp - 1 + n_tp - 1 + n_tp // 2)
+
+    for k, d in enumerate((1, -1)):
+        remote(heads, hall.at[t], sent.at[6], asem.at[k], s, side(d)).start()
+    loads[0].wait()
+
+    width = heads.shape[1]
+
+    def project(x, q):
+        return jnp.dot(x, oc[pl.ds(pl.multiple_of(q * width, width), width)], preferred_element_type=f32)
+
+    stream[...] = stream_in[...].astype(f32) + project(heads[...], t)
+    for k, d in enumerate((-1, 1)):
+        arrived(hall.at[side(d)], asem.at[k])
+        ref = hall.at[side(d), pl.ds(k * half, half)]
+        remote(ref, ref, sent.at[7], a2sem.at[k], s, side(-d)).start()
+    stream[...] += project(hall[side(-1)], side(-1)) + project(hall[side(1)], side(1))
+    for k in range(2):
+        arrived(hall.at[side(2), pl.ds(k * half, half)], a2sem.at[k])
+    total = stream[...] + project(hall[side(2)], side(2))
+    stream[...] = total
+
+    part = jnp.sum(total * total, axis=1, keepdims=True)
+    ssq[t] = jnp.broadcast_to(part, (rows, 128)).T[:8]
+    for d in range(1, n_tp):
+        remote(ssq.at[t], ssq.at[t], sent.at[8], qsem.at[d], s, side(d)).start()
+    for d in range(1, n_tp):
+        arrived(ssq.at[side(-d)], qsem.at[d])
+    sums = ssq[0]
+    for q in range(1, n_tp):
+        sums = sums + ssq[q]
+    inv = lax.rsqrt(sums / (feats * n_tp) + EPS)
+    inv = jnp.concatenate([inv] * 16, axis=0).T[:, :1]
+    normed = (stream[...] * inv * gain[...]).astype(bf)
+
+    own = pltpu.make_async_copy(send.at[s], xbuf.at[t, s], local_sem.at[0])
+
+    def pack(j):
+        plane = to_plane(j)
+        place = plane * (group * cap) + lax.broadcasted_iota(jnp.int32, (group * cap, rows), 0)
+        chosen = (place == slots_row[0:1]) | (place == slots_row[1:2])
+        picked = jnp.dot(jnp.where(chosen, 1.0, 0.0).astype(bf), normed, preferred_element_type=f32)
+        send[pl.ds(pl.multiple_of(plane * group, group), group)] = picked.astype(bf).reshape(group, cap, feats)
+        return plane
+
+    pack(0)
+    own.start()
+
+    def near(i, c):
+        dest = z * group + lax.rem(w + i, group)
+        remote(send.at[dest], xbuf.at[t, s], sent.at[0], dsem.at[0], dest, t).start()
+        return c
+
+    lax.fori_loop(1, group, near, 0)
+
+    def far(j, c):
+        plane = pack(j)
+
+        def one(i, c):
+            dest = plane * group + lax.rem(w + i, group)
+            remote(send.at[dest], xbuf.at[t, s], sent.at[0], dsem.at[j], dest, t).start()
+            return c
+
+        return lax.fori_loop(0, group, one, c)
+
+    lax.fori_loop(1, n_z, far, 0)
+    for load in loads[1:]:
+        load.wait()
+
+    def chunk(q, j):
+        return xbuf.at[q, pl.ds(from_plane(j) * group, group)]
+
+    def stage_x(j):
+        @pl.when(j == 0)
+        def _():
+            own.wait()
+            arrived(xbuf.at[t, pl.ds(0, group - 1)], dsem.at[0])
+
+        @pl.when(j > 0)
+        def _():
+            arrived(chunk(t, j), dsem.at[j])
+
+        for k, d in enumerate((1, -1)):
+            remote(chunk(t, j), chunk(t, j), sent.at[1], xsem.at[k, j], s, side(d)).start()
+
+    def stage_x2(j):
+        arrived(chunk(side(-1), j), xsem.at[0, j])
+        arrived(chunk(side(1), j), xsem.at[1, j])
+        d = 1 - 2 * lax.rem(j, 2)
+        ref = chunk(side(-d), j)
+        remote(ref, ref, sent.at[2], x2sem.at[j], s, side(d)).start()
+
+    def stage_up(j):
+        arrived(chunk(side(2), j), x2sem.at[j])
+        first = pl.multiple_of(from_plane(j) * group, group)
+        gate = jnp.zeros((group * cap, units), f32)
+        upper = jnp.zeros((group * cap, units), f32)
+        for q in range(n_tp):
+            x = xbuf[q, pl.ds(first, group)].reshape(group * cap, feats)
+            gate = gate + jnp.dot(x, gate_w[q * feats : (q + 1) * feats], preferred_element_type=f32)
+            upper = upper + jnp.dot(x, up_w[q * feats : (q + 1) * feats], preferred_element_type=f32)
+        act = gate / (1.0 + jnp.exp(-gate)) * upper
+        plane = from_plane(j)
+        hbuf[t, plane] = act.astype(bf)
+        for k, d in enumerate((1, -1)):
+            ref = hbuf.at[t, plane]
+            remote(ref, ref, sent.at[3], hsem.at[k, j], s, side(d)).start()
+
+    def stage_h2(j):
+        plane = from_plane(j)
+        arrived(hbuf.at[side(-1), plane], hsem.at[0, j])
+        arrived(hbuf.at[side(1), plane], hsem.at[1, j])
+        d = 1 - 2 * lax.rem(j, 2)
+        ref = hbuf.at[side(-d), plane]
+        remote(ref, ref, sent.at[4], h2sem.at[j], s, side(d)).start()
+
+    def stage_down(j):
+        plane = from_plane(j)
+        arrived(hbuf.at[side(2), plane], h2sem.at[j])
+        res = jnp.zeros((group * cap, feats), f32)
+        for q in range(n_tp):
+            res = res + jnp.dot(hbuf[q, plane], down_w[q * units : (q + 1) * units], preferred_element_type=f32)
+        first = pl.multiple_of(plane * group, group)
+        rbuf[pl.ds(first, group)] = res.astype(bf).reshape(group, cap, feats)
+
+        @pl.when(j == 0)
+        def _():
+            pltpu.make_async_copy(rbuf.at[s], back.at[s], local_sem.at[1]).start()
+
+            def one(i, c):
+                dest = z * group + lax.rem(w + i, group)
+                remote(rbuf.at[dest], back.at[s], sent.at[5], bsem.at[0], dest, t).start()
+                return c
+
+            lax.fori_loop(1, group, one, 0)
+
+        @pl.when(j > 0)
+        def _():
+            def one(i, c):
+                dest = plane * group + lax.rem(w + i, group)
+                remote(rbuf.at[dest], back.at[s], sent.at[5], bsem.at[j], dest, t).start()
+                return c
+
+            lax.fori_loop(0, group, one, 0)
+
+    stages = (stage_x, stage_x2, stage_up, stage_h2, stage_down)
+
+    def step(i, c):
+        for lag, stage in enumerate(stages):
+            j = i - lag
+
+            @pl.when((j >= 0) & (j < n_z))
+            def _():
+                stage(j)
+
+        return c
+
+    lax.fori_loop(0, n_z + len(stages) - 1, step, 0)
+
+    pltpu.make_async_copy(rbuf.at[s], back.at[s], local_sem.at[1]).wait()
+    arrived(back.at[pl.ds(0, group - 1)], bsem.at[0])
+
+    def home(j, c):
+        arrived(back.at[pl.ds(to_plane(j) * group, group)], bsem.at[j])
+        return c
+
+    lax.fori_loop(1, n_z, home, 0)
+
+    table = back[...].reshape(n_sp * cap, feats)
+    total = stream[...]
+    place = lax.broadcasted_iota(jnp.int32, (rows, n_sp * cap), 1)
+    for k in range(2):
+        chosen = jnp.where(place == slots_col[:, k : k + 1], 1.0, 0.0).astype(bf)
+        total = total + route[:, k : k + 1] * jnp.dot(chosen, table, preferred_element_type=f32)
+    mix[...] = total.astype(bf)
+    columns = out.at[:, pl.ds(pl.multiple_of(t * feats, feats), feats)]
+    for b in range(n_tp):
+        piece = mix.at[pl.ds(b * block, block)]
+        if b < n_tp // 2:
+
+            @pl.when(t == b)
+            def _():
+                pltpu.make_async_copy(piece, columns, local_sem.at[2]).start()
+
+            @pl.when(t != b)
+            def _():
+                remote(piece, columns, sent.at[9], fsem.at[t], s, b).start()
+        else:
+            remote(piece, columns, sent.at[9], fsem.at[t], far_s, b).start()
+    for q in range(n_tp):
+        ref = out.at[:, pl.ds(q * feats, feats)]
+        mine = (t == q) & low
+
+        @pl.when(mine)
+        def _():
+            pltpu.make_async_copy(mix.at[pl.ds(0, block)], ref, local_sem.at[2]).wait()
+
+        @pl.when(jnp.logical_not(mine))
+        def _():
+            arrived(ref, fsem.at[q])
+
+    left(send.at[pl.ds(0, n_sp - 1)], sent.at[0])
+    left(xbuf.at[pl.ds(0, 2)], sent.at[1])
+    left(xbuf.at[0], sent.at[2])
+    left(hbuf.at[pl.ds(0, 2)], sent.at[3])
+    left(hbuf.at[0], sent.at[4])
+    left(rbuf.at[pl.ds(0, n_sp - 1)], sent.at[5])
+    left(hall.at[pl.ds(0, 2)], sent.at[6])
+    left(hall.at[0], sent.at[7])
+    left(ssq.at[pl.ds(0, n_tp - 1)], sent.at[8])
+
+    @pl.when(low)
+    def _():
+        left(mix.at[pl.ds(0, (n_tp - 1) * block)], sent.at[9])
+
+    @pl.when(jnp.logical_not(low))
+    def _():
+        left(mix, sent.at[9])
+
+
+def post(heads, out_w, stream_in, gain, slots_row, slots_col, route, gate_w, up_w, down_w, n_sp, n_tp, group, cap):
+    rows, feats = stream_in.shape
+    units = gate_w.shape[1]
+    n_z = n_sp // group
+    bf, f32 = jnp.bfloat16, jnp.float32
+    dma = pltpu.SemaphoreType.DMA
+    vmem, hbm = pl.BlockSpec(memory_space=pltpu.VMEM), pl.BlockSpec(memory_space=pl.ANY)
+    return pl.pallas_call(
+        functools.partial(post_kernel, n_sp, n_tp, group),
+        out_shape=jax.ShapeDtypeStruct((rows // n_tp, feats * n_tp), bf),
+        in_specs=[vmem, hbm, vmem, vmem, vmem, vmem, vmem, hbm, hbm, hbm],
+        out_specs=vmem,
+        scratch_shapes=[
+            pltpu.VMEM((n_tp,) + heads.shape, bf),
+            pltpu.VMEM(out_w.shape, bf),
+            pltpu.VMEM(gate_w.shape, bf),
+            pltpu.VMEM(up_w.shape, bf),
+            pltpu.VMEM(down_w.shape, bf),
+            pltpu.VMEM((rows, feats), f32),
+            pltpu.VMEM((n_tp, 8, rows), f32),
+            pltpu.VMEM((n_sp, cap, feats), bf),
+            pltpu.VMEM((n_tp, n_sp, cap, feats), bf),
+            pltpu.VMEM((n_tp, n_z, group * cap, units), bf),
+            pltpu.VMEM((n_sp, cap, feats), bf),
+            pltpu.VMEM((n_sp, cap, feats), bf),
+            pltpu.VMEM((rows, feats), bf),
+            dma((10,)), dma((3,)), dma((4,)), dma((2,)), dma((2,)), dma((n_tp,)), dma((n_z,)), dma((2, n_z)),
+            dma((n_z,)), dma((2, n_z)), dma((n_z,)), dma((n_z,)), dma((n_tp,)),
+        ],
+        compiler_params=pltpu.CompilerParams(
+            collective_id=1, has_side_effects=True, vmem_limit_bytes=40 * 1024 * 1024),
+        name="post",
+    )(heads, out_w, stream_in, gain, slots_row, slots_col, route, gate_w, up_w, down_w)
+
+
 def shards(
     stream_in, queries_one, queries_two, keys_one, keys_two, values, lambdas, head_gain, out_weight,
     norm_gain, expert_ids, route_weight, gate_weight, up_weight, down_weight,
@@ -106,7 +427,7 @@
     q_all = jnp.stack([q_pair[:, :half], q_far])
     q_all = q_all.reshape(2, 2, half, 2, HEAD_DIM).transpose(0, 1, 3, 2, 4).reshape(2, 2, rows, HEAD_DIM)
     stream_far = lax.ppermute(stream_in, ("sp", "tp"), home)
-    stream_mine = lax.all_to_all(stream_far, "tp", 1, 0, tiled=True).astype(f32)
+    stream_mine = lax.all_to_all(stream_far, "tp", 1, 0, tiled=True)
     ids = lax.all_gather(lax.ppermute(expert_ids, ("sp", "tp"), home), "tp", axis=0, tiled=True)
     route = lax.all_gather(lax.ppermute(route_weight, ("sp", "tp"), home), "tp", axis=0, tiled=True)
     out_cols = lax.all_to_all(out_weight, "tp", 1, 0, tiled=True)
@@ -120,31 +441,13 @@
     before = jnp.dot(lower, one_hot, preferred_element_type=f32)
     ranks = jnp.sum(before * one_hot.astype(f32), axis=1).astype(jnp.int32)
     slots = (flat * cap + ranks).reshape(rows, 2)
-    pick = [(slots[:, k][:, None] == lax.iota(jnp.int32, n_sp * cap)[None, :]).astype(bf) for k in range(2)]
-
     packed = jnp.concatenate([keys_one, keys_two, values], 1)
     kv = lax.all_gather(packed, "sp", axis=0, tiled=True)
     heads = flash(q_all, kv, lambdas, head_gain[None], n_sp)
-    heads_all = lax.all_gather(heads, "tp", axis=1, tiled=True)
-    stream = stream_mine + jnp.dot(heads_all, out_cols, preferred_element_type=f32)
-    ssq = lax.psum(jnp.sum(stream * stream, axis=1), "tp")
-    inv = lax.rsqrt(ssq / (feats * n_tp) + EPS)
-    normed = (stream * inv[:, None] * gain_mine).astype(bf)
-    send = lax.dot_general(
-        pick[0] + pick[1], normed, (((0,), (0,)), ((), ())), preferred_element_type=f32
-    ).astype(bf)
-    got = lax.all_to_all(send, "sp", 0, 0, tiled=True)
-    got = lax.all_gather(got, "tp", axis=1, tiled=True)
-    gate = jnp.dot(got, gate_weight[0], preferred_element_type=f32)
-    upper = jnp.dot(got, up_weight[0], preferred_element_type=f32)
-    hidden = (jax.nn.silu(gate) * upper).astype(bf)
-    hidden = lax.all_gather(hidden, "tp", axis=1, tiled=True)
-    result = jnp.dot(hidden, down_cols, preferred_element_type=f32).astype(bf)
-    back = lax.all_to_all(result, "sp", 0, 0, tiled=True)
-    for k in range(2):
-        stream = stream + route[:, k][:, None] * jnp.dot(pick[k], back, preferred_element_type=f32)
-    mixed = lax.all_to_all(stream.astype(bf), "tp", 0, 1, tiled=True)
-    return lax.ppermute(mixed, ("sp", "tp"), home)
+    return post(
+        heads, out_cols, stream_mine, gain_mine[None], slots.T, slots, route, gate_weight[0], up_weight[0], down_cols,
+        n_sp, n_tp, n_sp // PLANES, cap,
+    )
 
 
 def solution(mesh):

time: 393 us -> 269 us (0.68)
  waiting for transfers between devices: 184 us -> 32.3 us
  Pallas kernels: 28.9 us -> 139 us
  blocking collectives: 85.3 us -> 13.8 us
  matrix products: 15.3 us -> 1.04 us
  local copies, waits for them, and re-layouts: 11.6 us -> 19.7 us
  starting transfers between devices: 47.1 us -> 42.6 us
    pallas_call x0 -> x1, Pallas kernels: none -> 111 us  [post(): pl.pallas_call(functools.partial(post_kernel, n_sp, n_tp, group), out_sha...]
    all_gather x3 -> x0, waiting for transfers between devices: 66.8 us -> none  [the longest x1 45.6 us: shards(): got = lax.all_gather(got, 'tp', axis=1, tiled=True)]
    all_to_all x3 -> x0, blocking collectives: 66.8 us -> none  [the longest x1 40.6 us: shards(): got = lax.all_to_all(send, 'sp', 0, 0, tiled=True)]
    all_gather x1, waiting for transfers between devices: 62.7 us -> 6.8 us  [shards(): kv = lax.all_gather(packed, 'sp', axis=0, tiled=True)]
    ppermute x1, waiting for transfers between devices: 19.4 us -> 0.01 us  [shards(): lax.ppermute(route_weight, ('sp', 'tp'), home)]
    dot_general x7 -> x0, matrix products: 15 us -> none  [the longest x1 3.82 us: shards(): result = jnp.dot(hidden, down_cols, preferred_element_type=f32).astype(bf)]
    ppermute x1 -> x0, waiting for transfers between devices: 14.1 us -> none  [shards(): return lax.ppermute(mixed, ('sp', 'tp'), home)]
    all_to_all x2, waiting for transfers between devices: 0.43 us -> 12.1 us  [the longest x1 10.1 us: shards(): down_cols = lax.all_to_all(down_weight[0], 'tp', 1, 0, tiled=True)]
  transfers between devices with their start and end apart: 12 -> 8, of which waited for: 8 -> 4; matrix products, arithmetic and copies ran while one was open for 3% -> 7% of each run, Pallas kernels for 7% -> 11%
where the time goes in v2:
time: 269 us; the launch traced here: 268 us
  Pallas kernels  139 us (52%)
  starting transfers between devices  42.6 us (16%)
  waiting for transfers between devices  32.3 us (12%)
  local copies, waits for them, and re-layouts  19.7 us (7%)
  blocking collectives  13.8 us (5%)
  between operations  13.5 us (5%)
  other arithmetic  6.06 us (2%)
    pallas_call x1, Pallas kernels, post(): pl.pallas_call(functools.partial(post_kernel, n_sp, n_tp, group), out_sha...  111 us
    pallas_call x1, Pallas kernels, flash(): pl.pallas_call(functools.partial(flash_kernel, n_sp), out_shape=jax.Shape...  28.2 us
    ppermute x1, waiting for transfers between devices, shards(): stream_far = lax.ppermute(stream_in, ('sp', 'tp'), home)  13.4 us
    ppermute x1, starting transfers between devices, shards(): stream_far = lax.ppermute(stream_in, ('sp', 'tp'), home)  10.5 us
    all_to_all x1, waiting for transfers between devices, shards(): down_cols = lax.all_to_all(down_weight[0], 'tp', 1, 0, tiled=True)  10.1 us
    all_gather x1, blocking collectives, shards(): lax.all_gather(lax.ppermute(route_weight, ('sp', 'tp'), home), 'tp', axis...  8.44 us
    ppermute x1, starting transfers between devices, shards(): q_far = lax.ppermute(q_pair[:, half:], 'sp', mirror)  8.16 us
    ppermute x1, starting transfers between devices, shards(): lax.ppermute(route_weight, ('sp', 'tp'), home)  6.97 us
  transfers between devices with their start and end apart: 8, of which 4 were waited for; matrix products, arithmetic and copies ran while one was open for 7% of the time, Pallas kernels for 11%

profile of v2, /device:TPU:7, one launch (start us, length us, event | category | flops | bytes accessed | tf_op | source)
XLA Modules:
  0.0 268.0 jit_solution(11262059801542627192)
XLA Ops:
  6.5 1.7 pad_maximum_fusion.1
  8.3 10.5 %collective-permute-start.1 = (bf16[64,2048]{1,0:T(8,128)(2,1)}, bf16[64,2048]{1,0:T(8,128)(2,1)S(1)}, u32[]{:S(2)}, u32[]{:S(2)}) collective-permute-start(bf16[64,2048]{1,0:T(8,128)(2,1)} %param.15), channel_id=1, source_target_pairs={{0,0},{1,1},{2,254},{3,255},{4,4},{5,5},{6,250},{7,251},{8,8},{9,9... | collective-permute-start | bytes 786440 | tf_op jit(solution)/shard_map/ppermute | solution.py:429
  18.8 13.4 %collective-permute-done.1 = bf16[64,2048]{1,0:T(8,128)(2,1)S(1)} collective-permute-done((bf16[64,2048]{1,0:T(8,128)(2,1)}, bf16[64,2048]{1,0:T(8,128)(2,1)S(1)}, u32[]{:S(2)}, u32[]{:S(2)}) %collective-permute-start.1) | collective-permute-done | bytes 262176 | tf_op jit(solution)/shard_map/ppermute | solution.py:429
  33.0 4.2 %all-to-all-start.1 = ((bf16[64,4,512]{2,0,1:T(8,128)(2,1)}), bf16[64,4,512]{2,0,1:T(8,128)(2,1)S(1)}, u32[]{:S(2)}, u32[]{:S(2)}) async-start(bf16[64,4,512]{2,0,1:T(8,128)(2,1)} %bitcast.31), calls=%async_computation.1 | async-start | bytes 524288 | tf_op jit(solution)/shard_map/all_to_all | solution.py:430
  38.0 1.2 copy.50
  39.2 2.0 all-to-all-done.1
  41.2 5.3 %all-to-all-start.2 = ((bf16[256,4,512]{2,0,1:T(8,128)(2,1)}), bf16[256,4,512]{2,0,1:T(8,128)(2,1)S(1)}, u32[]{:S(2)}, u32[]{:S(2)}) async-start(bf16[256,4,512]{2,0,1:T(8,128)(2,1)} %copy.50), calls=%async_computation.2 | async-start | bytes 2097152 | tf_op jit(solution)/shard_map/all_to_all | solution.py:434
  46.5 1.5 copy.57
  48.0 10.1 %all-to-all-done.2 = bf16[256,4,512]{2,0,1:T(8,128)(2,1)S(1)} async-done(((bf16[256,4,512]{2,0,1:T(8,128)(2,1)}), bf16[256,4,512]{2,0,1:T(8,128)(2,1)S(1)}, u32[]{:S(2)}, u32[]{:S(2)}) %all-to-all-start.2) | async-done | bytes 1048608 | tf_op jit(solution)/shard_map/all_to_all | solution.py:434
  58.1 5.5 %all-to-all-start = ((bf16[512,4,512]{2,0,1:T(8,128)(2,1)}), bf16[512,4,512]{2,0,1:T(8,128)(2,1)S(1)}, u32[]{:S(2)}, u32[]{:S(2)}) async-start(bf16[512,4,512]{2,0,1:T(8,128)(2,1)} %bitcast.42), calls=%async_computation | async-start | bytes 4194304 | tf_op jit(solution)/shard_map/all_to_all | solution.py:433
  63.6 1.7 fusion.1
  65.3 8.2 %collective-permute-start = (bf16[2,128,256]{2,1,0:T(8,128)(2,1)}, bf16[2,128,256]{2,1,0:T(8,128)(2,1)}, u32[]{:S(2)}, u32[]{:S(2)}) collective-permute-start(bf16[2,128,256]{2,1,0:T(8,128)(2,1)} %get-tuple-element.6), channel_id=1, source_target_pairs={{0,252},{4,248},{8,244},{12,240},{16,236},{20,232},{24,228},{28,22... | collective-permute-start | bytes 393224 | tf_op jit(solution)/shard_map/ppermute | solution.py:426
  73.5 1.9 collective-permute-start.2
  75.4 7.0 %collective-permute-start.3 = (f32[64,2]{0,1:T(2,128)}, f32[64,2]{0,1:T(2,128)}, u32[]{:S(2)}, u32[]{:S(2)}) collective-permute-start(f32[64,2]{0,1:T(2,128)} %param.26), channel_id=1, source_target_pairs={{0,0},{1,1},{2,254},{3,255},{4,4},{5,5},{6,250},{7,251},{8,8},{9,9... | collective-permute-start | bytes 1544 | tf_op jit(solution)/shard_map/ppermute | solution.py:432
  84.7 5.4 %all-gather = s32[4,64,2]{1,2,0:T(2,128)S(1)} all-gather(s32[1,64,2]{1,2,0:T(2,128)S(1)} %bitcast.47), channel_id=1, replica_groups=mesh['sp'=64,'tp'=4] {'tp'}, dimensions={0}, use_global_device_ids=true | all-gather | bytes 2560 | tf_op jit(solution)/shard_map/all_gather | solution.py:431
  94.7 8.4 %all-gather.1 = f32[4,64,2]{1,2,0:T(2,128)} all-gather(f32[1,64,2]{1,2,0:T(2,128)} %bitcast.13), channel_id=1, replica_groups=mesh['sp'=64,'tp'=4] {'tp'}, dimensions={0}, use_global_device_ids=true | all-gather | bytes 2560 | tf_op jit(solution)/shard_map/all_gather | solution.py:432
  103.1 1.4 copy.49
  104.6 1.6 stack.22
  107.1 1.6 pad_maximum_fusion
  108.7 6.8 %all-gather.4.cloned.1.call-done.kv_ref = bf16[16384,512]{1,0:T(8,128)(2,1)} async-done(((bf16[256,512]{1,0:T(8,128)(2,1)}), bf16[16384,512]{1,0:T(8,128)(2,1)}) %all-gather.4.cloned.1.call-update) | async-done | bytes 16777232 | tf_op jit(solution)/shard_map/all_gather | solution.py:445
  116.5 28.2 %flash.1.heads = bf16[256,512]{1,0:T(8,128)(2,1)S(1)} custom-call(bf16[2,2,256,128]{3,2,1,0:T(8,128)(2,1)S(1)} %bitcast.38, bf16[16384,512]{1,0:T(8,128)(2,1)} %all-gather.4.cloned.1.call-done.kv_ref, f32[2]{0:T(128)S(1)} %copy-done.7, f32[1,256]{1,0:T(1,128)S(1)} %bitcast.41), custom_call_target="tpu_custom_call" | custom-call | tf_op jit(solution)/shard_map/flash/pallas_call | solution.py:69
  145.4 1.2 copy-done
  146.6 1.2 copy-done.1
  149.7 110.7 %post.1 = bf16[64,2048]{1,0:T(8,128)(2,1)S(1)} custom-call(bf16[256,512]{1,0:T(8,128)(2,1)S(1)} %copy-done.4, bf16[2048,512]{1,0:T(8,128)(2,1)S(1)} %bitcast.32, bf16[256,512]{1,0:T(8,128)(2,1)S(1)} %bitcast.37, f32[1,512]{1,0:T(1,128)S(1)} %bitcast.40, s32[2,256]{1,0:T(2,128)S(1)} %copy.51.slots_row, s32[256,2]{1,0:T(8,128)S(1)} %bitcast_add_fusion.slots_col, ...), custom_call_target="tpu_custom_call" | custom-call | tf_op jit(solution)/shard_map/post/pallas_call | solution.py:381
  (44 shorter events, 13.6 us)
Async XLA Ops:
  6.5 30.6 %copy-start.9 = (bf16[1,256,2048]{2,1,0:T(8,128)(2,1)S(1)}, bf16[1,256,2048]{2,1,0:T(8,128)(2,1)}, u32[]{:S(2)}) copy-start(bf16[1,256,2048]{2,1,0:T(8,128)(2,1)} %param.29) | copy-start | bytes 3145732
  6.5 109.0 %all-gather.4.cloned.1.call-start = ((), (), s32[]{:S(2)}) async-start(), calls=%async_computation.3 | async-start | bytes 17039360 | tf_op jit(solution)/shard_map/all_gather | solution.py:445
  8.3 23.9 %collective-permute-start.1 = (bf16[64,2048]{1,0:T(8,128)(2,1)}, bf16[64,2048]{1,0:T(8,128)(2,1)S(1)}, u32[]{:S(2)}, u32[]{:S(2)}) collective-permute-start(bf16[64,2048]{1,0:T(8,128)(2,1)} %param.15), channel_id=1, source_target_pairs={{0,0},{1,1},{2,254},{3,255},{4,4},{5,5},{6,250},{7,251},{8,8},{9,9... | collective-permute-start | bytes 786440 | tf_op jit(solution)/shard_map/ppermute | solution.py:429
  33.0 8.2 %all-to-all-start.1 = ((bf16[64,4,512]{2,0,1:T(8,128)(2,1)}), bf16[64,4,512]{2,0,1:T(8,128)(2,1)S(1)}, u32[]{:S(2)}, u32[]{:S(2)}) async-start(bf16[64,4,512]{2,0,1:T(8,128)(2,1)} %bitcast.31), calls=%async_computation.1 | async-start | bytes 524288 | tf_op jit(solution)/shard_map/all_to_all | solution.py:430
  38.0 8.5 %copy-start.8 = (bf16[512,2048]{1,0:T(8,128)(2,1)S(1)}, bf16[512,2048]{1,0:T(8,128)(2,1)}, u32[]{:S(2)}) copy-start(bf16[512,2048]{1,0:T(8,128)(2,1)} %param.23) | copy-start | bytes 6291460
  41.2 16.9 %all-to-all-start.2 = ((bf16[256,4,512]{2,0,1:T(8,128)(2,1)}), bf16[256,4,512]{2,0,1:T(8,128)(2,1)S(1)}, u32[]{:S(2)}, u32[]{:S(2)}) async-start(bf16[256,4,512]{2,0,1:T(8,128)(2,1)} %copy.50), calls=%async_computation.2 | async-start | bytes 2097152 | tf_op jit(solution)/shard_map/all_to_all | solution.py:434
  58.1 5.5 %copy-start.10 = (bf16[256,256]{1,0:T(8,128)(2,1)S(1)}, bf16[256,256]{1,0:T(8,128)(2,1)}, u32[]{:S(2)}) copy-start(bf16[256,256]{1,0:T(8,128)(2,1)} %param.16) | copy-start | bytes 393220
  58.1 15.4 %copy-start.11 = (s32[64,2]{0,1:T(2,128)S(1)}, s32[64,2]{0,1:T(2,128)}, u32[]{:S(2)}) copy-start(s32[64,2]{0,1:T(2,128)} %param.25) | copy-start | bytes 1540
  58.1 87.3 %all-to-all-start = ((bf16[512,4,512]{2,0,1:T(8,128)(2,1)}), bf16[512,4,512]{2,0,1:T(8,128)(2,1)S(1)}, u32[]{:S(2)}, u32[]{:S(2)}) async-start(bf16[512,4,512]{2,0,1:T(8,128)(2,1)} %bitcast.42), calls=%async_computation | async-start | bytes 4194304 | tf_op jit(solution)/shard_map/all_to_all | solution.py:433
  63.6 51.9 %copy-start.6 = (f32[256]{0:T(256)S(1)}, f32[256]{0:T(256)}, u32[]{:S(2)}) copy-start(f32[256]{0:T(256)} %param.22) | copy-start | bytes 3076
  63.6 51.9 %copy-start.7 = (f32[2]{0:T(128)S(1)}, f32[2]{0:T(128)}, u32[]{:S(2)}) copy-start(f32[2]{0:T(128)} %lam_ref.1) | copy-start | bytes 28
  65.3 39.3 %collective-permute-start = (bf16[2,128,256]{2,1,0:T(8,128)(2,1)}, bf16[2,128,256]{2,1,0:T(8,128)(2,1)}, u32[]{:S(2)}, u32[]{:S(2)}) collective-permute-start(bf16[2,128,256]{2,1,0:T(8,128)(2,1)} %get-tuple-element.6), channel_id=1, source_target_pairs={{0,252},{4,248},{8,244},{12,240},{16,236},{20,232},{24,228},{28,22... | collective-permute-start | bytes 393224 | tf_op jit(solution)/shard_map/ppermute | solution.py:426
  73.5 11.3 %collective-permute-start.2 = (s32[64,2]{0,1:T(2,128)S(1)}, s32[64,2]{0,1:T(2,128)S(1)}, u32[]{:S(2)}, u32[]{:S(2)}) collective-permute-start(s32[64,2]{0,1:T(2,128)S(1)} %copy-done.11), channel_id=1, source_target_pairs={{0,0},{1,1},{2,254},{3,255},{4,4},{5,5},{6,250},{7,251},{8,8},{9,9... | collective-permute-start | bytes 1544 | tf_op jit(solution)/shard_map/ppermute | solution.py:431
  75.4 19.3 %collective-permute-start.3 = (f32[64,2]{0,1:T(2,128)}, f32[64,2]{0,1:T(2,128)}, u32[]{:S(2)}, u32[]{:S(2)}) collective-permute-start(f32[64,2]{0,1:T(2,128)} %param.26), channel_id=1, source_target_pairs={{0,0},{1,1},{2,254},{3,255},{4,4},{5,5},{6,250},{7,251},{8,8},{9,9... | collective-permute-start | bytes 1544 | tf_op jit(solution)/shard_map/ppermute | solution.py:432
  115.5 1.0 copy-start.2
  144.7 0.7 copy-start.3
  145.4 1.2 copy-start
  146.6 1.2 copy-start.1
  147.8 0.9 copy-start.4
  148.8 0.9 copy-start.5
Sparse Core Ops, SparseCore 0:
  10.1 105.3 all-gather.3

commit v3 on v2

--- a/solution.py
+++ b/solution.py
@@ -13,84 +13,385 @@
 EPS = 1e-06
 OUT_SCALE = 0.8
 SCALE2 = HEAD_DIM ** (-0.5) * math.log2(math.e)
-BK = 1024
-PLANES = 8
-
-
-def flash_kernel(n_sp, q_ref, kv_ref, lam_ref, gain_ref, out_ref, m_ref, l_ref, acc_ref):
-    me = lax.axis_index("sp")
-    rows = q_ref.shape[2]
-    half = rows // 2
-
-    def update(run, block, masked, first_row):
-        start = pl.multiple_of(block * BK, BK)
-        v = kv_ref[pl.ds(start, BK), 2 * HEAD_DIM :]
+MESH = pl.DeviceIdType.MESH
+CHIPS = (8, 4, 2)
+SPLIT = 144
+CAP = 16
+
+
+def front_kernel(dims, queries_one, queries_two, keys_one, keys_two, values, stream_in, meta_in, out_w, down_w, lam, gain,
+                 heads, stream, meta, out_cols, down_cols, kv, q_far, q_all, m_ref, l_ref, acc_ref,
+                 sent, local_sem, qsem, ssem, msem, osem, wsem, pz, py, py2, ry, ry2, rz, sib):
+    n_z, n_y, n_c, n_tp, split = dims
+    n_sp = n_z * n_y * n_c
+    s, t = lax.axis_index("sp"), lax.axis_index("tp")
+    c = lax.rem(s, n_c)
+    y = lax.rem(s // n_c, n_y)
+    z = s // (n_c * n_y)
+    far_s = n_sp - 1 - s
+    rows = queries_one.shape[0]
+    half, block = rows // 2, rows // n_tp
+    feats = stream.shape[1]
+    turn = n_z // 2
+    n_keys = n_y // 2 * n_c * rows
+    f32, bf = jnp.float32, jnp.bfloat16
+
+    def sp_of(zz, yy, cc):
+        return (zz * n_y + yy) * n_c + cc
+
+    def zn(d):
+        return lax.rem(z + d + n_z, n_z)
+
+    def yn(d):
+        return lax.rem(y + d + n_y, n_y)
+
+    def tn(d):
+        return lax.rem(t + d, n_tp)
+
+    def remote(src, dst, a, b, sp, tp):
+        return pltpu.make_async_remote_copy(
+            src_ref=src, dst_ref=dst, send_sem=a, recv_sem=b, device_id=(sp, tp), device_id_type=MESH)
+
+    def arrived(ref, sem):
+        remote(ref, ref, sent.at[0], sem, far_s, t).wait_recv()
+
+    def left(ref, sem):
+        remote(ref, ref, sem, qsem.at[0], far_s, t).wait_send()
+
+    mine = kv.at[z, y, c]
+    own = [
+        pltpu.make_async_copy(keys_one, mine.at[:, pl.ds(0, HEAD_DIM)], local_sem.at[0]),
+        pltpu.make_async_copy(keys_two, mine.at[:, pl.ds(HEAD_DIM, HEAD_DIM)], local_sem.at[1]),
+        pltpu.make_async_copy(values, mine.at[:, pl.ds(2 * HEAD_DIM, VAL_DIM)], local_sem.at[2]),
+    ]
+    for copy in own:
+        copy.start()
+
+    barrier = pltpu.get_barrier_semaphore()
+
+    def hello(sp, tp):
+        pl.semaphore_signal(barrier, inc=1, device_id=(sp, tp), device_id_type=MESH)
+
+    hello(sp_of(z, y, 1 - c), t)
+    for d in (1, -1):
+        hello(sp_of(zn(d), y, c), t)
+        hello(sp_of(z, yn(d), c), t)
+    for d in range(1, n_tp):
+        hello(s, tn(d))
+    hello(far_s, t)
+    for q in range(n_tp // 2, n_tp):
+        hello(far_s, q)
+    high = t // (n_tp // 2)
+    pl.semaphore_wait(barrier, 5 + n_tp + high * n_tp)
+    for copy in own:
+        copy.wait()
+
+    def lower(zz, yy):
+        return kv.at[zz, yy, c, pl.ds(0, split)]
+
+    def upper(zz, yy):
+        return kv.at[zz, yy, c, pl.ds(split, rows - split)]
+
+    def to_z(ref, d, a, sem):
+        remote(ref, ref, sent.at[a], sem, sp_of(zn(d), y, c), t).start()
+
+    def to_y(ref, d, a, sem):
+        remote(ref, ref, sent.at[a], sem, sp_of(z, yn(d), c), t).start()
+
+    for k, d in enumerate((1, -1)):
+        to_z(lower(z, y), d, 0, pz.at[k, 1])
+        to_y(upper(z, y), d, 1, ry.at[k])
+    for i, queries in enumerate((queries_one, queries_two)):
+        remote(queries.at[pl.ds(half, half)], q_far.at[i], sent.at[2], qsem.at[i], far_s, t).start()
+    for k, d in enumerate((1, -1)):
+        to_z(upper(z, y), d, 3, rz.at[0, k, 1])
+        to_y(lower(z, y), d, 4, py.at[0, k])
+
+    sp_home = jnp.where(high == 1, far_s, s)
+    slab = stream.at[pl.ds(pl.multiple_of(t * block, block), block)]
+    for q in range(n_tp):
+        piece = stream_in.at[:, pl.ds(q * feats, feats)]
+        at_home = (t == q) & (high == 0)
+
+        @pl.when(at_home)
+        def _():
+            pltpu.make_async_copy(piece, slab, local_sem.at[3]).start()
+            pltpu.make_async_copy(meta_in, meta.at[t], local_sem.at[4]).start()
+
+        @pl.when(jnp.logical_not(at_home))
+        def _():
+            remote(meta_in, meta.at[t], sent.at[5], msem.at[t], sp_home, q).start()
+            remote(piece, slab, sent.at[6], ssem.at[t], sp_home, q).start()
+
+    depth, units = out_w.shape[0], down_w.shape[0]
+    out_rows = out_cols.at[pl.ds(pl.multiple_of(t * depth, depth), depth)]
+    down_rows = down_cols.at[pl.ds(pl.multiple_of(t * units, units), units)]
+
+    def strip(ref, q):
+        return ref.at[:, pl.ds(pl.multiple_of(q * feats, feats), feats)]
+
+    for d in range(1, n_tp):
+        remote(strip(down_w, tn(d)), down_rows, sent.at[7], wsem.at[d], s, tn(d)).start()
+        remote(strip(out_w, tn(d)), out_rows, sent.at[8], osem.at[d], s, tn(d)).start()
+    weights = [
+        pltpu.make_async_copy(strip(down_w, t), down_rows, local_sem.at[5]),
+        pltpu.make_async_copy(strip(out_w, t), out_rows, local_sem.at[6]),
+    ]
+    for copy in weights:
+        copy.start()
+
+    for k, d in enumerate((-1, 1)):
+        ref = upper(z, yn(d))
+        arrived(ref, ry.at[k])
+
+        @pl.when(c == k)
+        def _():
+            to_y(ref, -d, 9, ry2.at[0])
+
+        for kk, dd in enumerate((1, -1)):
+            to_z(ref, dd, 3, rz.at[1 + k, kk, 1])
+    ref = upper(z, yn(2))
+    arrived(ref, ry2.at[0])
+    for kk, dd in enumerate((1, -1)):
+        to_z(ref, dd, 3, rz.at[3, kk, 1])
+
+    m_ref[...] = jnp.full(m_ref.shape, -1e30, f32)
+    l_ref[...] = jnp.zeros(l_ref.shape, f32)
+    acc_ref[...] = jnp.zeros(acc_ref.shape, f32)
+
+    def plane(j):
+        return lax.rem(z + (j + 1) // 2 * (1 - 2 * lax.rem(j, 2)) + n_z, n_z)
+
+    def goes(h, k):
+        return (h < turn) | ((h == turn) & (c == k))
+
+    def each_plane(h, f):
+        for a in range(2):
+            j = jnp.where(h == 0, 0, jnp.minimum(2 * h - 1 + a, n_z - 1))
+
+            @pl.when((a == 0) | ((h >= 1) & (h < turn)))
+            def _():
+                f(j, plane(j))
+
+    def lower_arrives(h):
+        for k, d in enumerate((1, -1)):
+
+            @pl.when(goes(h, k))
+            def _():
+                zz = zn(-d * h)
+                ref = lower(zz, y)
+                arrived(ref, pz.at[k, h])
+
+                @pl.when(goes(h + 1, k))
+                def _():
+                    to_z(ref, d, 0, pz.at[k, h + 1])
+
+                j = jnp.minimum(2 * h - 1 + k, n_z - 1)
+                for kk, dd in enumerate((1, -1)):
+                    to_y(ref, dd, 4, py.at[j, kk])
+
+    def upper_arrives(h, r):
+        yy = lax.rem(y + jnp.where(r == 0, 0, jnp.where(r == 1, n_y - 1, jnp.where(r == 2, 1, 2))), n_y)
+        for k, d in enumerate((1, -1)):
+
+            @pl.when(goes(h, k))
+            def _():
+                ref = upper(zn(-d * h), yy)
+                arrived(ref, rz.at[r, k, h])
+
+                @pl.when(goes(h + 1, k))
+                def _():
+                    to_z(ref, d, 3, rz.at[r, k, h + 1])
+
+    def spread(j, zz):
+        arrived(lower(zz, yn(-1)), py.at[j, 0])
+        arrived(lower(zz, yn(1)), py.at[j, 1])
+        d = 1 - 2 * lax.rem(j, 2)
+        to_y(lower(zz, yn(-d)), d, 10, py2.at[j])
+
+    def share(j, zz):
+        arrived(lower(zz, yn(2)), py2.at[j])
+        ref = kv.at[zz, :, c]
+        remote(ref, ref, sent.at[11], sib.at[j], sp_of(z, y, 1 - c), t).start()
+
+    def update(run, zz, part, masked, first_row):
+        keys_all = kv[zz, pl.ds(part * (n_y // 2), n_y // 2)].reshape(n_keys, 2 * HEAD_DIM + VAL_DIM)
+        v = keys_all[:, 2 * HEAD_DIM :]
         if masked:
-            row = first_row + lax.rem(lax.broadcasted_iota(jnp.int32, (rows, BK), 0), half)
-            keep = start + lax.broadcasted_iota(jnp.int32, (rows, BK), 1) <= row
+            first_key = (zz * 2 + part) * n_keys
+            row = first_row + lax.rem(lax.broadcasted_iota(jnp.int32, (rows, n_keys), 0), half)
+            keep = first_key + lax.broadcasted_iota(jnp.int32, (rows, n_keys), 1) <= row
         for k in range(2):
-            q = q_ref[run, k]
-            keys = kv_ref[pl.ds(start, BK), k * HEAD_DIM : (k + 1) * HEAD_DIM]
-            s = lax.dot_general(q, keys, (((1,), (1,)), ((), ())), preferred_element_type=jnp.float32)
+            keys = keys_all[:, k * HEAD_DIM : (k + 1) * HEAD_DIM]
+            scores = lax.dot_general(q_all[run, k], keys, (((1,), (1,)), ((), ())), preferred_element_type=f32)
             if masked:
-                s = jnp.where(keep, s, -jnp.inf)
-            old = m_ref[k]
-            new = jnp.maximum(old, jnp.max(s, axis=1, keepdims=True))
-            terms = jnp.exp2((s - new[:, :1]) * SCALE2)
+                scores = jnp.where(keep, scores, -jnp.inf)
+            old = m_ref[run, k]
+            new = jnp.maximum(old, jnp.max(scores, axis=1, keepdims=True))
+            terms = jnp.exp2((scores - new[:, :1]) * SCALE2)
             fade = jnp.exp2((old - new) * SCALE2)
-            part = terms[:, :128]
-            for c in range(1, BK // 128):
-                part = part + terms[:, c * 128 : (c + 1) * 128]
-            m_ref[k] = new
-            l_ref[k] = l_ref[k] * fade + part
-            acc_ref[k] = acc_ref[k] * fade[:, :1] + jnp.dot(
-                terms.astype(jnp.bfloat16), v, preferred_element_type=jnp.float32
-            )
+            lanes = terms[:, :128]
+            for i in range(1, n_keys // 128):
+                lanes = lanes + terms[:, i * 128 : (i + 1) * 128]
+            m_ref[run, k] = new
+            l_ref[run, k] = l_ref[run, k] * fade + lanes
+            acc_ref[run, k] = acc_ref[run, k] * fade[:, :1] + jnp.dot(terms.astype(bf), v, preferred_element_type=f32)
+
+    def row_of(run):
+        return jnp.where(run == 0, s * rows, far_s * rows + half)
+
+    def attend(j, part):
+        zz = plane(j)
+
+        @pl.when(part == 0)
+        def _():
+            arrived(kv.at[zz, :, 1 - c], sib.at[j])
+
+        def one(run, carry):
+            here, last = zz * 2 + part, row_of(run) // n_keys
+
+            @pl.when(here < last)
+            def _():
+                update(run, zz, part, False, row_of(run))
+
+            @pl.when(here == last)
+            def _():
+                update(run, zz, part, True, row_of(run))
+
+            return carry
+
+        lax.fori_loop(0, 2, one, 0)
+
+    def step(u, carry):
+        h, sub = u // 5, lax.rem(u, 5)
+
+        @pl.when((sub == 0) & (h <= turn))
+        def _():
+            lower_arrives(h)
+
+        @pl.when(sub == 0)
+        def _():
+            each_plane(h - 1, spread)
+
+        @pl.when((sub > 0) & (h <= turn))
+        def _():
+            upper_arrives(h, sub - 1)
+
+        @pl.when(sub == 2)
+        def _():
+            each_plane(h - 1, share)
+
+        @pl.when(u == 8)
+        def _():
+            for i, queries in enumerate((queries_one, queries_two)):
+                arrived(q_far.at[i], qsem.at[i])
+                for g in range(2):
+                    place = pl.ds(g * half, half)
+                    lanes = slice(g * HEAD_DIM, (g + 1) * HEAD_DIM)
+                    q_all[0, i, place] = queries[:half, lanes]
+                    q_all[1, i, place] = q_far[i, :, lanes]
+
+        v = u - 8
+        hc, i = v // 5, lax.rem(v, 5)
+        j = jnp.where(hc == 0, 0, jnp.minimum(2 * hc - 1 + i // 2, n_z - 1))
+
+        @pl.when((v >= 0) & ((i < 2) | ((i < 4) & (hc > 0) & (hc < turn))))
+        def _():
+            attend(j, lax.rem(i, 2))
+
+        return carry
+
+    lax.fori_loop(5, 5 * (turn + 2), step, 0)
 
     for run in range(2):
-        first_row = me * 2 * half if run == 0 else (n_sp - 1 - me) * 2 * half + half
-        m_ref[...] = jnp.full(m_ref.shape, -1e30, jnp.float32)
-        l_ref[...] = jnp.zeros(l_ref.shape, jnp.float32)
-        acc_ref[...] = jnp.zeros(acc_ref.shape, jnp.float32)
-        full = first_row // BK
-        lax.fori_loop(0, full, lambda i, c: (update(run, i, False, first_row), c)[1], 0)
-        update(run, full, True, first_row)
-        mix = [acc_ref[k] / jnp.sum(l_ref[k], axis=1, keepdims=True) for k in range(2)]
-        for h in range(2):
-            piece = slice(h * half, (h + 1) * half)
-            diff = mix[0][piece] - lam_ref[h] * mix[1][piece]
+        mix = [acc_ref[run, k] / jnp.sum(l_ref[run, k], axis=1, keepdims=True) for k in range(2)]
+        for g in range(2):
+            piece = slice(g * half, (g + 1) * half)
+            diff = mix[0][piece] - lam[g] * mix[1][piece]
             ms = jnp.mean(diff * diff, axis=1, keepdims=True)
-            res = diff * lax.rsqrt(ms + EPS) * gain_ref[...] * OUT_SCALE
-            out_ref[run * half : (run + 1) * half, h * VAL_DIM : (h + 1) * VAL_DIM] = res.astype(jnp.bfloat16)
-
-
-def flash(q, kv, lambdas, gain, n_sp):
-    rows = q.shape[2]
+            res = diff * lax.rsqrt(ms + EPS) * gain[...] * OUT_SCALE
+            heads[run * half : (run + 1) * half, g * VAL_DIM : (g + 1) * VAL_DIM] = res.astype(bf)
+
+    for q in range(n_tp):
+        ref = stream.at[pl.ds(q * block, block)]
+        at_home = (t == q) & (high == 0)
+
+        @pl.when(at_home)
+        def _():
+            pltpu.make_async_copy(stream_in.at[:, pl.ds(q * feats, feats)], ref, local_sem.at[3]).wait()
+            pltpu.make_async_copy(meta_in, meta.at[q], local_sem.at[4]).wait()
+
+        @pl.when(jnp.logical_not(at_home))
+        def _():
+            arrived(ref, ssem.at[q])
+            arrived(meta.at[q], msem.at[q])
+
+    for copy in weights:
+        copy.wait()
+    for d in range(1, n_tp):
+        arrived(down_rows, wsem.at[d])
+        arrived(out_rows, osem.at[d])
+    left(kv.at[pl.ds(0, n_z - 1), 0, 0, pl.ds(0, split)], sent.at[0])
+    left(kv.at[0, pl.ds(0, 2), 0, pl.ds(split, rows - split)], sent.at[1])
+    left(q_far, sent.at[2])
+    left(kv.at[pl.ds(0, n_z - 1), :, 0, pl.ds(split, rows - split)], sent.at[3])
+    left(kv.at[:, pl.ds(0, 2), 0, pl.ds(0, split)], sent.at[4])
+    left(kv.at[0, 0, 0, pl.ds(split, rows - split)], sent.at[9])
+    left(kv.at[:, 0, 0, pl.ds(0, split)], sent.at[10])
+    left(kv.at[:, :, 0], sent.at[11])
+    for d in range(1, n_tp):
+        left(down_rows, sent.at[7])
+        left(out_rows, sent.at[8])
+
+    @pl.when(high == 0)
+    def _():
+        left(meta.at[pl.ds(0, n_tp - 1)], sent.at[5])
+        left(stream.at[pl.ds(0, (n_tp - 1) * block)], sent.at[6])
+
+    @pl.when(high == 1)
+    def _():
+        left(meta, sent.at[5])
+        left(stream, sent.at[6])
+
+
+def front(queries_one, queries_two, keys_one, keys_two, values, stream_in, meta, out_w, down_w, lam, gain, dims):
+    n_z, n_y, n_c, n_tp, split = dims
+    rows = queries_one.shape[0]
+    feats = stream_in.shape[1] // n_tp
+    turn = n_z // 2
+    bf, f32 = jnp.bfloat16, jnp.float32
+    dma = pltpu.SemaphoreType.DMA
+    vmem, hbm = pl.BlockSpec(memory_space=pltpu.VMEM), pl.BlockSpec(memory_space=pl.ANY)
+    smem = pl.BlockSpec(memory_space=pltpu.SMEM)
     return pl.pallas_call(
-        functools.partial(flash_kernel, n_sp),
-        out_shape=jax.ShapeDtypeStruct((rows, 2 * VAL_DIM), jnp.bfloat16),
-        in_specs=[
-            pl.BlockSpec(memory_space=pltpu.VMEM),
-            pl.BlockSpec(memory_space=pltpu.VMEM),
-            pl.BlockSpec(memory_space=pltpu.SMEM),
-            pl.BlockSpec(memory_space=pltpu.VMEM),
+        functools.partial(front_kernel, dims),
+        out_shape=(
+            jax.ShapeDtypeStruct((rows, 2 * VAL_DIM), bf),
+            jax.ShapeDtypeStruct((rows, feats), bf),
+            jax.ShapeDtypeStruct((n_tp,) + meta.shape, f32),
+            jax.ShapeDtypeStruct((n_tp * out_w.shape[0], feats), bf),
+            jax.ShapeDtypeStruct((n_tp * down_w.shape[0], feats), bf),
+        ),
+        in_specs=[vmem, vmem, hbm, hbm, hbm, vmem, vmem, hbm, hbm, smem, vmem],
+        out_specs=(vmem, vmem, vmem, hbm, hbm),
+        scratch_shapes=[
+            pltpu.VMEM((n_z, n_y, n_c, rows, 2 * HEAD_DIM + VAL_DIM), bf),
+            pltpu.VMEM((2, rows // 2, 2 * HEAD_DIM), bf),
+            pltpu.VMEM((2, 2, rows, HEAD_DIM), bf),
+            pltpu.VMEM((2, 2, rows, 128), f32),
+            pltpu.VMEM((2, 2, rows, 128), f32),
+            pltpu.VMEM((2, 2, rows, VAL_DIM), f32),
+            dma((12,)), dma((7,)), dma((2,)), dma((n_tp,)), dma((n_tp,)), dma((n_tp,)), dma((n_tp,)),
+            dma((2, turn + 1)), dma((n_z, 2)), dma((n_z,)), dma((2,)), dma((1,)), dma((4, 2, turn + 1)), dma((n_z,)),
         ],
-        out_specs=pl.BlockSpec(memory_space=pltpu.VMEM),
-        scratch_shapes=[
-            pltpu.VMEM((2, rows, 128), jnp.float32),
-            pltpu.VMEM((2, rows, 128), jnp.float32),
-            pltpu.VMEM((2, rows, VAL_DIM), jnp.float32),
-        ],
-        compiler_params=pltpu.CompilerParams(vmem_limit_bytes=48 * 1024 * 1024),
-        name="flash",
-    )(q, kv, lambdas, gain)
-
-
-MESH = pl.DeviceIdType.MESH
-
-
-def post_kernel(n_sp, n_tp, group, heads, out_w, stream_in, gain, slots_row, slots_col, route, gate_h, up_h, down_h,
-                out, hall, oc, gate_w, up_w, down_w, stream, ssq, send, xbuf, hbuf, rbuf, back, mix,
+        compiler_params=pltpu.CompilerParams(
+            collective_id=0, has_side_effects=True, vmem_limit_bytes=48 * 1024 * 1024),
+        name="front",
+    )(queries_one, queries_two, keys_one, keys_two, values, stream_in, meta, out_w, down_w, lam, gain)
+
+
+def post_kernel(n_sp, n_tp, group, heads, out_w, stream_in, gain, meta, gate_h, up_h, down_h,
+                out, hall, slots_row, slots_col, oc, gate_w, up_w, down_w, stream, ssq, send, xbuf, hbuf, rbuf, back, mix,
                 sent, local_sem, wsem, asem, a2sem, qsem, dsem, xsem, x2sem, hsem, h2sem, bsem, fsem):
     s, t = lax.axis_index("sp"), lax.axis_index("tp")
     n_z = n_sp // group
@@ -155,6 +456,21 @@
 
     for k, d in enumerate((1, -1)):
         remote(heads, hall.at[t], sent.at[6], asem.at[k], s, side(d)).start()
+
+    base = jnp.concatenate([jnp.concatenate([meta[q]] * 16, axis=0).T[:block] for q in range(n_tp)], axis=0)
+    lane = lax.broadcasted_iota(jnp.int32, (rows, 128), 1)
+    earlier = lax.broadcasted_iota(jnp.int32, (rows, rows), 1) < lax.broadcasted_iota(jnp.int32, (rows, rows), 0)
+    earlier = jnp.where(earlier, 1.0, 0.0).astype(bf)
+    taken = jnp.zeros((1, 128), f32)
+    places = base
+    for k in range(2):
+        named = jnp.where(lane.astype(f32) == base[:, k : k + 1], 1.0, 0.0)
+        before = jnp.dot(earlier, named.astype(bf), preferred_element_type=f32) + taken
+        rank = jnp.sum(before * named, axis=1, keepdims=True)
+        taken = taken + jnp.sum(named, axis=0, keepdims=True)
+        places = jnp.where(lane == k, base[:, k : k + 1] * cap + rank, places)
+    slots_col[...] = places
+    slots_row[...] = places.T[:8]
     loads[0].wait()
 
     width = heads.shape[1]
@@ -184,14 +500,15 @@
         sums = sums + ssq[q]
     inv = lax.rsqrt(sums / (feats * n_tp) + EPS)
     inv = jnp.concatenate([inv] * 16, axis=0).T[:, :1]
-    normed = (stream[...] * inv * gain[...]).astype(bf)
+    normed = (stream[...] * inv * gain[:, pl.ds(pl.multiple_of(t * feats, feats), feats)]).astype(bf)
 
     own = pltpu.make_async_copy(send.at[s], xbuf.at[t, s], local_sem.at[0])
 
     def pack(j):
         plane = to_plane(j)
         place = plane * (group * cap) + lax.broadcasted_iota(jnp.int32, (group * cap, rows), 0)
-        chosen = (place == slots_row[0:1]) | (place == slots_row[1:2])
+        place = place.astype(f32)
+        chosen = (place == slots_row[0:1, :]) | (place == slots_row[1:2, :])
         picked = jnp.dot(jnp.where(chosen, 1.0, 0.0).astype(bf), normed, preferred_element_type=f32)
         send[pl.ds(pl.multiple_of(plane * group, group), group)] = picked.astype(bf).reshape(group, cap, feats)
         return plane
@@ -321,10 +638,10 @@
 
     table = back[...].reshape(n_sp * cap, feats)
     total = stream[...]
-    place = lax.broadcasted_iota(jnp.int32, (rows, n_sp * cap), 1)
+    place = lax.broadcasted_iota(jnp.int32, (rows, n_sp * cap), 1).astype(f32)
     for k in range(2):
         chosen = jnp.where(place == slots_col[:, k : k + 1], 1.0, 0.0).astype(bf)
-        total = total + route[:, k : k + 1] * jnp.dot(chosen, table, preferred_element_type=f32)
+        total = total + slots_col[:, 2 + k : 3 + k] * jnp.dot(chosen, table, preferred_element_type=f32)
     mix[...] = total.astype(bf)
     columns = out.at[:, pl.ds(pl.multiple_of(t * feats, feats), feats)]
     for b in range(n_tp):
@@ -371,7 +688,7 @@
         left(mix, sent.at[9])
 
 
-def post(heads, out_w, stream_in, gain, slots_row, slots_col, route, gate_w, up_w, down_w, n_sp, n_tp, group, cap):
+def post(heads, out_w, stream_in, gain, meta, gate_w, up_w, down_w, n_sp, n_tp, group, cap):
     rows, feats = stream_in.shape
     units = gate_w.shape[1]
     n_z = n_sp // group
@@ -381,10 +698,12 @@
     return pl.pallas_call(
         functools.partial(post_kernel, n_sp, n_tp, group),
         out_shape=jax.ShapeDtypeStruct((rows // n_tp, feats * n_tp), bf),
-        in_specs=[vmem, hbm, vmem, vmem, vmem, vmem, vmem, hbm, hbm, hbm],
+        in_specs=[vmem, hbm, vmem, vmem, vmem, hbm, hbm, hbm],
         out_specs=vmem,
         scratch_shapes=[
             pltpu.VMEM((n_tp,) + heads.shape, bf),
+            pltpu.VMEM((8, rows), f32),
+            pltpu.VMEM((rows, 128), f32),
             pltpu.VMEM(out_w.shape, bf),
             pltpu.VMEM(gate_w.shape, bf),
             pltpu.VMEM(up_w.shape, bf),
@@ -403,7 +722,7 @@
         compiler_params=pltpu.CompilerParams(
             collective_id=1, has_side_effects=True, vmem_limit_bytes=40 * 1024 * 1024),
         name="post",
-    )(heads, out_w, stream_in, gain, slots_row, slots_col, route, gate_w, up_w, down_w)
+    )(heads, out_w, stream_in, gain, meta, gate_w, up_w, down_w)
 
 
 def shards(
@@ -411,42 +730,15 @@
     norm_gain, expert_ids, route_weight, gate_weight, up_weight, down_weight,
 ):
     n_sp, n_tp = lax.axis_size("sp"), lax.axis_size("tp")
-    rows = queries_one.shape[0]
-    half = rows // 2
-    feats = stream_in.shape[1] // n_tp
-    bf, f32 = jnp.bfloat16, jnp.float32
-
-    mirror = [(s, n_sp - 1 - s) for s in range(n_sp)]
-    home = [
-        (s * n_tp + t, (s if t < n_tp // 2 else n_sp - 1 - s) * n_tp + t)
-        for s in range(n_sp)
-        for t in range(n_tp)
-    ]
-    q_pair = jnp.stack([queries_one, queries_two])
-    q_far = lax.ppermute(q_pair[:, half:], "sp", mirror)
-    q_all = jnp.stack([q_pair[:, :half], q_far])
-    q_all = q_all.reshape(2, 2, half, 2, HEAD_DIM).transpose(0, 1, 3, 2, 4).reshape(2, 2, rows, HEAD_DIM)
-    stream_far = lax.ppermute(stream_in, ("sp", "tp"), home)
-    stream_mine = lax.all_to_all(stream_far, "tp", 1, 0, tiled=True)
-    ids = lax.all_gather(lax.ppermute(expert_ids, ("sp", "tp"), home), "tp", axis=0, tiled=True)
-    route = lax.all_gather(lax.ppermute(route_weight, ("sp", "tp"), home), "tp", axis=0, tiled=True)
-    out_cols = lax.all_to_all(out_weight, "tp", 1, 0, tiled=True)
-    down_cols = lax.all_to_all(down_weight[0], "tp", 1, 0, tiled=True)
-    gain_mine = lax.dynamic_slice_in_dim(norm_gain, lax.axis_index("tp") * feats, feats, 0)
-
-    cap = 16
-    flat = ids.reshape(-1)
-    one_hot = (flat[:, None] == lax.iota(jnp.int32, n_sp)[None, :]).astype(bf)
-    lower = (lax.iota(jnp.int32, 2 * rows)[:, None] > lax.iota(jnp.int32, 2 * rows)[None, :]).astype(bf)
-    before = jnp.dot(lower, one_hot, preferred_element_type=f32)
-    ranks = jnp.sum(before * one_hot.astype(f32), axis=1).astype(jnp.int32)
-    slots = (flat * cap + ranks).reshape(rows, 2)
-    packed = jnp.concatenate([keys_one, keys_two, values], 1)
-    kv = lax.all_gather(packed, "sp", axis=0, tiled=True)
-    heads = flash(q_all, kv, lambdas, head_gain[None], n_sp)
+    meta = jnp.concatenate([expert_ids.astype(jnp.float32), route_weight], 1).T
+    meta = jnp.pad(meta, ((0, 8 - meta.shape[0]), (0, 128 - meta.shape[1])))
+    heads, stream, meta, out_cols, down_cols = front(
+        queries_one, queries_two, keys_one, keys_two, values, stream_in, meta, out_weight, down_weight[0],
+        lambdas, head_gain[None], CHIPS + (n_tp, SPLIT),
+    )
     return post(
-        heads, out_cols, stream_mine, gain_mine[None], slots.T, slots, route, gate_weight[0], up_weight[0], down_cols,
-        n_sp, n_tp, n_sp // PLANES, cap,
+        heads, out_cols, stream, norm_gain[None], meta, gate_weight[0], up_weight[0], down_cols,
+        n_sp, n_tp, n_sp // CHIPS[0], CAP,
     )
 
 

time: 269 us -> 235 us (0.87)
  Pallas kernels: 139 us -> 225 us
  starting transfers between devices: 42.6 us -> 0 us
  waiting for transfers between devices: 32.3 us -> 0 us
  blocking collectives: 13.8 us -> 0 us
  between operations: 13.5 us -> 0.06 us
  local copies, waits for them, and re-layouts: 19.7 us -> 8.61 us
  other arithmetic: 6.06 us -> 1.38 us
    pallas_call x1, Pallas kernels: 28.2 us -> 101 us  [front(): pl.pallas_call(functools.partial(front_kernel, dims), out_shape=(jax.Shap...]
    ppermute x4 -> x0, starting transfers between devices: 27.5 us -> none  [the longest x1 10.5 us: shards(): stream_far = lax.ppermute(stream_in, ('sp', 'tp'), home)]
    all_to_all x3 -> x0, starting transfers between devices: 15 us -> none  [the longest x1 5.5 us: shards(): out_cols = lax.all_to_all(out_weight, 'tp', 1, 0, tiled=True)]
    all_gather x2 -> x0, blocking collectives: 13.8 us -> none  [the longest x1 8.44 us: shards(): lax.all_gather(lax.ppermute(route_weight, ('sp', 'tp'), home), 'tp', axis...]
    ppermute x4 -> x0, waiting for transfers between devices: 13.4 us -> none  [the longest x1 13.4 us: shards(): stream_far = lax.ppermute(stream_in, ('sp', 'tp'), home)]
    pallas_call x1, Pallas kernels: 111 us -> 124 us  [post(): pl.pallas_call(functools.partial(post_kernel, n_sp, n_tp, group), out_sha...]
    all_to_all x3 -> x0, waiting for transfers between devices: 12.1 us -> none  [the longest x1 10.1 us: shards(): down_cols = lax.all_to_all(down_weight[0], 'tp', 1, 0, tiled=True)]
    all_gather x1 -> x0, waiting for transfers between devices: 6.8 us -> none  [shards(): kv = lax.all_gather(packed, 'sp', axis=0, tiled=True)]
  transfers between devices with their start and end apart: 8 -> 0, of which waited for: 4 -> 0; matrix products, arithmetic and copies ran while one was open for 7% -> 0% of each run, Pallas kernels for 11% -> 0%
where the time goes in v3:
time: 235 us
  Pallas kernels  225 us (96%)
  local copies, waits for them, and re-layouts  8.61 us (4%)
    pallas_call x1, Pallas kernels, post(): pl.pallas_call(functools.partial(post_kernel, n_sp, n_tp, group), out_sha...  124 us
    pallas_call x1, Pallas kernels, front(): pl.pallas_call(functools.partial(front_kernel, dims), out_shape=(jax.Shap...  101 us
    unnamed x25, local copies, waits for them, and re-layouts  8.61 us

profile of v3, /device:TPU:7, one launch (start us, length us, event | category | flops | bytes accessed | tf_op | source)
XLA Modules:
  0.0 234.9 jit_solution(9216782416598307686)
XLA Ops:
  0.0 0.0 copy-start.9
  0.0 0.7 convert_element_type.5
  0.7 0.7 maximum_bitcast_fusion
  1.4 0.0 copy-start
  1.4 1.2 copy-done
  2.6 0.9 copy-done.3
  3.6 0.0 copy-start.4
  3.6 0.9 copy-done.4
  4.5 0.0 copy-start.5
  4.5 0.9 copy-done.5
  5.4 0.9 copy-done.6
  6.3 0.0 copy-start.7
  6.3 0.8 copy-done.7
  7.1 0.0 copy-start.8
  7.1 0.8 copy-done.8
  8.0 0.0 copy-start.10
  8.0 0.7 copy-done.10
  8.6 0.7 copy-done.11
  9.3 100.7 %front.1 = (bf16[256,512]{1,0:T(8,128)(2,1)S(1)}, bf16[256,512]{1,0:T(8,128)(2,1)S(1)}, f32[4,8,128]{2,1,0:T(8,128)S(1)}, bf16[2048,512]{1,0:T(8,128)(2,1)S(1)}, bf16[1024,512]{1,0:T(8,128)(2,1)S(1)}) custom-call(bf16[256,256]{1,0:T(8,128)(2,1)S(1)} %copy-done.4, bf16[256,256]{1,0:T(8,128)(2,1)S(1)} %copy-done.5, bf16[256,128]{1,0:T(8,128)(2,1)S(1)} %copy-done.7, ...), custom_call_target="tpu_custom_call" | custom-call | tf_op jit(solution)/shard_map/front/pallas_call | solution.py:366
  110.0 0.0 copy-done.9
  110.0 0.0 copy-done.1
  110.0 0.0 copy-done.2
  110.1 124.1 %post.1 = bf16[64,2048]{1,0:T(8,128)(2,1)S(1)} custom-call(bf16[256,512]{1,0:T(8,128)(2,1)S(1)} %get-tuple-element.10.heads, bf16[2048,512]{1,0:T(8,128)(2,1)S(1)} %get-tuple-element.11.out_w, bf16[256,512]{1,0:T(8,128)(2,1)S(1)} %get-tuple-element.12.stream_in, f32[1,2048]{1,0:T(1,128)S(1)} %bitcast.10, f32[4,8,128]{2,1,0:T(8,128)S(1)} %get-tuple-element.13.meta, ...), custom_call_target="tpu_custom_call" | custom-call | tf_op jit(solution)/shard_map/post/pallas_call | solution.py:698
  234.1 0.7 copy.17
  (6 shorter events, 0.0 us)
Async XLA Ops:
  0.0 110.0 %copy-start.9 = (f32[2048]{0:T(1024)S(1)}, f32[2048]{0:T(1024)}, u32[]{:S(2)}) copy-start(f32[2048]{0:T(1024)} %param.24) | copy-start | bytes 24580
  1.4 1.2 copy-start
  2.6 0.9 copy-start.3
  3.6 0.9 copy-start.4
  4.5 0.9 copy-start.5
  5.4 0.9 copy-start.6
  6.3 0.8 copy-start.7
  7.1 0.8 copy-start.8
  8.0 0.7 copy-start.10
  8.6 0.7 copy-start.11
  9.3 100.7 %copy-start.1 = (bf16[1,2048,256]{2,1,0:T(8,128)(2,1)S(1)}, bf16[1,2048,256]{2,1,0:T(8,128)(2,1)}, u32[]{:S(2)}) copy-start(bf16[1,2048,256]{2,1,0:T(8,128)(2,1)} %param.27) | copy-start | bytes 3145732
  9.3 100.7 %copy-start.2 = (bf16[1,2048,256]{2,1,0:T(8,128)(2,1)S(1)}, bf16[1,2048,256]{2,1,0:T(8,128)(2,1)}, u32[]{:S(2)}) copy-start(bf16[1,2048,256]{2,1,0:T(8,128)(2,1)} %param.28) | copy-start | bytes 3145732

commit v4 on v3

--- a/solution.py
+++ b/solution.py
@@ -17,6 +17,7 @@
 CHIPS = (8, 4, 2)
 SPLIT = 144
 CAP = 16
+LAST = 14
 
 
 def front_kernel(dims, queries_one, queries_two, keys_one, keys_two, values, stream_in, meta_in, out_w, down_w, lam, gain,
@@ -109,19 +110,21 @@
 
     sp_home = jnp.where(high == 1, far_s, s)
     slab = stream.at[pl.ds(pl.multiple_of(t * block, block), block)]
-    for q in range(n_tp):
-        piece = stream_in.at[:, pl.ds(q * feats, feats)]
-        at_home = (t == q) & (high == 0)
-
-        @pl.when(at_home)
-        def _():
-            pltpu.make_async_copy(piece, slab, local_sem.at[3]).start()
-            pltpu.make_async_copy(meta_in, meta.at[t], local_sem.at[4]).start()
-
-        @pl.when(jnp.logical_not(at_home))
-        def _():
-            remote(meta_in, meta.at[t], sent.at[5], msem.at[t], sp_home, q).start()
-            remote(piece, slab, sent.at[6], ssem.at[t], sp_home, q).start()
+
+    def send_rows():
+        for q in range(n_tp):
+            piece = stream_in.at[:, pl.ds(q * feats, feats)]
+            at_home = (t == q) & (high == 0)
+
+            @pl.when(at_home)
+            def _():
+                pltpu.make_async_copy(piece, slab, local_sem.at[3]).start()
+                pltpu.make_async_copy(meta_in, meta.at[t], local_sem.at[4]).start()
+
+            @pl.when(jnp.logical_not(at_home))
+            def _():
+                remote(meta_in, meta.at[t], sent.at[5], msem.at[t], sp_home, q).start()
+                remote(piece, slab, sent.at[6], ssem.at[t], sp_home, q).start()
 
     depth, units = out_w.shape[0], down_w.shape[0]
     out_rows = out_cols.at[pl.ds(pl.multiple_of(t * depth, depth), depth)]
@@ -240,48 +243,68 @@
     def row_of(run):
         return jnp.where(run == 0, s * rows, far_s * rows + half)
 
-    def attend(j, part):
-        zz = plane(j)
-
-        @pl.when(part == 0)
-        def _():
-            arrived(kv.at[zz, :, 1 - c], sib.at[j])
-
-        def one(run, carry):
-            here, last = zz * 2 + part, row_of(run) // n_keys
-
-            @pl.when(here < last)
-            def _():
-                update(run, zz, part, False, row_of(run))
-
-            @pl.when(here == last)
-            def _():
-                update(run, zz, part, True, row_of(run))
-
-            return carry
-
-        lax.fori_loop(0, 2, one, 0)
-
-    def step(u, carry):
+    def blocks(run, j):
+        return jnp.clip(row_of(run) // n_keys - 2 * plane(j) + 1, 0, 2)
+
+    def attend(n, u):
+        at, base = jnp.int32(0), jnp.int32(0)
+        count = jnp.int32(0)
+        for j in range(n_z):
+            count = count + blocks(0, j) + blocks(1, j)
+            passed = count <= n
+            at = at + jnp.where(passed, 1, 0)
+            base = jnp.where(passed, count, base)
+        at = jnp.minimum(at, n_z - 1)
+        i = n - base
+        short = blocks(0, at)
+        run = jnp.where(i < short, 0, 1)
+        part = i - jnp.where(i < short, 0, short)
+        zz = plane(at)
+
+        ready = (n < 2 * n_z + 1) & (u >= 5 * ((at + 1) // 2) + 7)
+
+        @pl.when(ready & (i == 0))
+        def _():
+            arrived(kv.at[zz, :, 1 - c], sib.at[at])
+
+        here, last = zz * 2 + part, row_of(run) // n_keys
+
+        @pl.when(ready & (here < last))
+        def _():
+            update(run, zz, part, False, row_of(run))
+
+        @pl.when(ready & (here == last))
+        def _():
+            update(run, zz, part, True, row_of(run))
+
+        return n + jnp.where(ready, 1, 0)
+
+    spread(jnp.int32(0), z)
+
+    def step(u, done):
         h, sub = u // 5, lax.rem(u, 5)
 
         @pl.when((sub == 0) & (h <= turn))
         def _():
             lower_arrives(h)
 
-        @pl.when(sub == 0)
-        def _():
-            each_plane(h - 1, spread)
-
         @pl.when((sub > 0) & (h <= turn))
         def _():
             upper_arrives(h, sub - 1)
 
-        @pl.when(sub == 2)
+        @pl.when((sub == 3) & (h <= turn))
+        def _():
+            each_plane(h, spread)
+
+        @pl.when((sub == 1) & (h <= turn + 1))
         def _():
             each_plane(h - 1, share)
 
-        @pl.when(u == 8)
+        @pl.when(u == 5 * turn)
+        def _():
+            send_rows()
+
+        @pl.when(u == 6)
         def _():
             for i, queries in enumerate((queries_one, queries_two)):
                 arrived(q_far.at[i], qsem.at[i])
@@ -291,17 +314,14 @@
                     q_all[0, i, place] = queries[:half, lanes]
                     q_all[1, i, place] = q_far[i, :, lanes]
 
-        v = u - 8
-        hc, i = v // 5, lax.rem(v, 5)
-        j = jnp.where(hc == 0, 0, jnp.minimum(2 * hc - 1 + i // 2, n_z - 1))
-
-        @pl.when((v >= 0) & ((i < 2) | ((i < 4) & (hc > 0) & (hc < turn))))
-        def _():
-            attend(j, lax.rem(i, 2))
-
-        return carry
-
-    lax.fori_loop(5, 5 * (turn + 2), step, 0)
+        return attend(done, u)
+
+    lax.fori_loop(5, 5 * turn + LAST, step, jnp.int32(0))
+    for j in range(1, n_z):
+
+        @pl.when(blocks(0, j) + blocks(1, j) == 0)
+        def _():
+            arrived(kv.at[plane(j), :, 1 - c], sib.at[j])
 
     for run in range(2):
         mix = [acc_ref[run, k] / jnp.sum(l_ref[run, k], axis=1, keepdims=True) for k in range(2)]
@@ -385,7 +405,7 @@
             dma((2, turn + 1)), dma((n_z, 2)), dma((n_z,)), dma((2,)), dma((1,)), dma((4, 2, turn + 1)), dma((n_z,)),
         ],
         compiler_params=pltpu.CompilerParams(
-            collective_id=0, has_side_effects=True, vmem_limit_bytes=48 * 1024 * 1024),
+            collective_id=0, has_side_effects=True, vmem_limit_bytes=60 * 1024 * 1024),
         name="front",
     )(queries_one, queries_two, keys_one, keys_two, values, stream_in, meta, out_w, down_w, lam, gain)
 
@@ -720,7 +740,7 @@
             dma((n_z,)), dma((2, n_z)), dma((n_z,)), dma((n_z,)), dma((n_tp,)),
         ],
         compiler_params=pltpu.CompilerParams(
-            collective_id=1, has_side_effects=True, vmem_limit_bytes=40 * 1024 * 1024),
+            collective_id=1, has_side_effects=True, vmem_limit_bytes=60 * 1024 * 1024),
         name="post",
     )(heads, out_w, stream_in, gain, meta, gate_w, up_w, down_w)
 

time: 235 us -> 201 us (0.86)
  Pallas kernels: 225 us -> 197 us
  local copies, waits for them, and re-layouts: 8.61 us -> 2.27 us
    pallas_call x1, Pallas kernels: 101 us -> 81.6 us  [front(): pl.pallas_call(functools.partial(front_kernel, dims), out_shape=(jax.Shap...]
    pallas_call x1, Pallas kernels: 124 us -> 116 us  [post(): pl.pallas_call(functools.partial(post_kernel, n_sp, n_tp, group), out_sha...]
    unnamed x25 -> x1, local copies, waits for them, and re-layouts: 8.61 us -> 1.67 us
where the time goes in v4:
time: 201 us
  Pallas kernels  197 us (98%)
  local copies, waits for them, and re-layouts  2.27 us (1%)
    pallas_call x1, Pallas kernels, post(): pl.pallas_call(functools.partial(post_kernel, n_sp, n_tp, group), out_sha...  116 us
    pallas_call x1, Pallas kernels, front(): pl.pallas_call(functools.partial(front_kernel, dims), out_shape=(jax.Shap...  81.6 us

profile of v4, /device:TPU:7, one launch (start us, length us, event | category | flops | bytes accessed | tf_op | source)
XLA Modules:
  0.0 200.9 jit_solution(6785152603484841274)
XLA Ops:
  0.0 0.7 convert_element_type.5
  0.7 0.7 maximum_bitcast_fusion
  1.4 0.6 pad.4.meta_in
  2.0 81.6 %front.1 = (bf16[256,512]{1,0:T(8,128)(2,1)}, bf16[256,512]{1,0:T(8,128)(2,1)}, f32[4,8,128]{2,1,0:T(8,128)}, bf16[2048,512]{1,0:T(8,128)(2,1)}, bf16[1024,512]{1,0:T(8,128)(2,1)}) custom-call(bf16[256,256]{1,0:T(8,128)(2,1)} %queries_one.1, bf16[256,256]{1,0:T(8,128)(2,1)} %queries_two.1, bf16[256,128]{1,0:T(8,128)(2,1)} %keys_one.1, ...), custom_call_target="tpu_custom_call" | custom-call | tf_op jit(solution)/shard_map/front/pallas_call | solution.py:386
  83.5 115.7 %post.1 = bf16[64,2048]{1,0:T(8,128)(2,1)} custom-call(bf16[256,512]{1,0:T(8,128)(2,1)} %get-tuple-element.10.heads, bf16[2048,512]{1,0:T(8,128)(2,1)} %get-tuple-element.11.out_w, bf16[256,512]{1,0:T(8,128)(2,1)} %get-tuple-element.12.stream_in, f32[1,2048]{1,0:T(1,128)} %bitcast.10, f32[4,8,128]{2,1,0:T(8,128)} %get-tuple-element.13.meta, ...), custom_call_target="tpu_custom_call" | custom-call | tf_op jit(solution)/shard_map/post/pallas_call | solution.py:718
  199.2 1.7 copy.17

commit v5 on v4

--- a/solution.py
+++ b/solution.py
@@ -18,11 +18,12 @@
 SPLIT = 144
 CAP = 16
 LAST = 14
-
-
-def front_kernel(dims, queries_one, queries_two, keys_one, keys_two, values, stream_in, meta_in, out_w, down_w, lam, gain,
-                 heads, stream, meta, out_cols, down_cols, kv, q_far, q_all, m_ref, l_ref, acc_ref,
-                 sent, local_sem, qsem, ssem, msem, osem, wsem, pz, py, py2, ry, ry2, rz, sib):
+N_FRONT = 19
+
+
+def attention_part(dims, queries_one, queries_two, keys_one, keys_two, values, meta_in, out_w, down_w, lam, gain,
+                 heads, meta, out_cols, down_cols, kv, q_far, q_all, m_ref, l_ref, acc_ref,
+                 sent, local_sem, qsem, msem, osem, wsem, pz, py, py2, ry, ry2, rz, sib):
     n_z, n_y, n_c, n_tp, split = dims
     n_sp = n_z * n_y * n_c
     s, t = lax.axis_index("sp"), lax.axis_index("tp")
@@ -31,8 +32,8 @@
     z = s // (n_c * n_y)
     far_s = n_sp - 1 - s
     rows = queries_one.shape[0]
-    half, block = rows // 2, rows // n_tp
-    feats = stream.shape[1]
+    half = rows // 2
+    feats = out_cols.shape[1]
     turn = n_z // 2
     n_keys = n_y // 2 * n_c * rows
     f32, bf = jnp.float32, jnp.bfloat16
@@ -73,17 +74,23 @@
     def hello(sp, tp):
         pl.semaphore_signal(barrier, inc=1, device_id=(sp, tp), device_id_type=MESH)
 
-    hello(sp_of(z, y, 1 - c), t)
-    for d in (1, -1):
-        hello(sp_of(zn(d), y, c), t)
-        hello(sp_of(z, yn(d), c), t)
+    def greet(o, carry):
+        hello(lax.rem(s + o, n_sp), t)
+        return carry
+
+    lax.fori_loop(1, n_sp, greet, 0)
     for d in range(1, n_tp):
         hello(s, tn(d))
-    hello(far_s, t)
+    high = t // (n_tp // 2)
+
+    @pl.when(high == 1)
+    def _():
+        for q in range(n_tp):
+            hello(far_s, q)
+
     for q in range(n_tp // 2, n_tp):
         hello(far_s, q)
-    high = t // (n_tp // 2)
-    pl.semaphore_wait(barrier, 5 + n_tp + high * n_tp)
+    pl.semaphore_wait(barrier, n_sp - 1 + n_tp - 1 + n_tp // 2 + n_tp * high)
     for copy in own:
         copy.wait()
 
@@ -109,22 +116,16 @@
         to_y(lower(z, y), d, 4, py.at[0, k])
 
     sp_home = jnp.where(high == 1, far_s, s)
-    slab = stream.at[pl.ds(pl.multiple_of(t * block, block), block)]
-
-    def send_rows():
-        for q in range(n_tp):
-            piece = stream_in.at[:, pl.ds(q * feats, feats)]
-            at_home = (t == q) & (high == 0)
-
-            @pl.when(at_home)
-            def _():
-                pltpu.make_async_copy(piece, slab, local_sem.at[3]).start()
-                pltpu.make_async_copy(meta_in, meta.at[t], local_sem.at[4]).start()
-
-            @pl.when(jnp.logical_not(at_home))
-            def _():
-                remote(meta_in, meta.at[t], sent.at[5], msem.at[t], sp_home, q).start()
-                remote(piece, slab, sent.at[6], ssem.at[t], sp_home, q).start()
+    for q in range(n_tp):
+        at_home = (t == q) & (high == 0)
+
+        @pl.when(at_home)
+        def _():
+            pltpu.make_async_copy(meta_in, meta.at[t], local_sem.at[4]).start()
+
+        @pl.when(jnp.logical_not(at_home))
+        def _():
+            remote(meta_in, meta.at[t], sent.at[5], msem.at[t], sp_home, q).start()
 
     depth, units = out_w.shape[0], down_w.shape[0]
     out_rows = out_cols.at[pl.ds(pl.multiple_of(t * depth, depth), depth)]
@@ -300,10 +301,6 @@
         def _():
             each_plane(h - 1, share)
 
-        @pl.when(u == 5 * turn)
-        def _():
-            send_rows()
-
         @pl.when(u == 6)
         def _():
             for i, queries in enumerate((queries_one, queries_two)):
@@ -333,17 +330,14 @@
             heads[run * half : (run + 1) * half, g * VAL_DIM : (g + 1) * VAL_DIM] = res.astype(bf)
 
     for q in range(n_tp):
-        ref = stream.at[pl.ds(q * block, block)]
         at_home = (t == q) & (high == 0)
 
         @pl.when(at_home)
         def _():
-            pltpu.make_async_copy(stream_in.at[:, pl.ds(q * feats, feats)], ref, local_sem.at[3]).wait()
             pltpu.make_async_copy(meta_in, meta.at[q], local_sem.at[4]).wait()
 
         @pl.when(jnp.logical_not(at_home))
         def _():
-            arrived(ref, ssem.at[q])
             arrived(meta.at[q], msem.at[q])
 
     for copy in weights:
@@ -366,53 +360,15 @@
     @pl.when(high == 0)
     def _():
         left(meta.at[pl.ds(0, n_tp - 1)], sent.at[5])
-        left(stream.at[pl.ds(0, (n_tp - 1) * block)], sent.at[6])
 
     @pl.when(high == 1)
     def _():
         left(meta, sent.at[5])
-        left(stream, sent.at[6])
-
-
-def front(queries_one, queries_two, keys_one, keys_two, values, stream_in, meta, out_w, down_w, lam, gain, dims):
-    n_z, n_y, n_c, n_tp, split = dims
-    rows = queries_one.shape[0]
-    feats = stream_in.shape[1] // n_tp
-    turn = n_z // 2
-    bf, f32 = jnp.bfloat16, jnp.float32
-    dma = pltpu.SemaphoreType.DMA
-    vmem, hbm = pl.BlockSpec(memory_space=pltpu.VMEM), pl.BlockSpec(memory_space=pl.ANY)
-    smem = pl.BlockSpec(memory_space=pltpu.SMEM)
-    return pl.pallas_call(
-        functools.partial(front_kernel, dims),
-        out_shape=(
-            jax.ShapeDtypeStruct((rows, 2 * VAL_DIM), bf),
-            jax.ShapeDtypeStruct((rows, feats), bf),
-            jax.ShapeDtypeStruct((n_tp,) + meta.shape, f32),
-            jax.ShapeDtypeStruct((n_tp * out_w.shape[0], feats), bf),
-            jax.ShapeDtypeStruct((n_tp * down_w.shape[0], feats), bf),
-        ),
-        in_specs=[vmem, vmem, hbm, hbm, hbm, vmem, vmem, hbm, hbm, smem, vmem],
-        out_specs=(vmem, vmem, vmem, hbm, hbm),
-        scratch_shapes=[
-            pltpu.VMEM((n_z, n_y, n_c, rows, 2 * HEAD_DIM + VAL_DIM), bf),
-            pltpu.VMEM((2, rows // 2, 2 * HEAD_DIM), bf),
-            pltpu.VMEM((2, 2, rows, HEAD_DIM), bf),
-            pltpu.VMEM((2, 2, rows, 128), f32),
-            pltpu.VMEM((2, 2, rows, 128), f32),
-            pltpu.VMEM((2, 2, rows, VAL_DIM), f32),
-            dma((12,)), dma((7,)), dma((2,)), dma((n_tp,)), dma((n_tp,)), dma((n_tp,)), dma((n_tp,)),
-            dma((2, turn + 1)), dma((n_z, 2)), dma((n_z,)), dma((2,)), dma((1,)), dma((4, 2, turn + 1)), dma((n_z,)),
-        ],
-        compiler_params=pltpu.CompilerParams(
-            collective_id=0, has_side_effects=True, vmem_limit_bytes=60 * 1024 * 1024),
-        name="front",
-    )(queries_one, queries_two, keys_one, keys_two, values, stream_in, meta, out_w, down_w, lam, gain)
-
-
-def post_kernel(n_sp, n_tp, group, heads, out_w, stream_in, gain, meta, gate_h, up_h, down_h,
-                out, hall, slots_row, slots_col, oc, gate_w, up_w, down_w, stream, ssq, send, xbuf, hbuf, rbuf, back, mix,
-                sent, local_sem, wsem, asem, a2sem, qsem, dsem, xsem, x2sem, hsem, h2sem, bsem, fsem):
+
+
+def experts_part(n_sp, n_tp, group, heads, rows_in, gain, meta, gate_h, up_h,
+                out, stream_in, hall, slots_row, slots_col, oc, gate_w, up_w, down_w, stream, ssq, send, xbuf, hbuf, rbuf, back, mix,
+                sent, local_sem, wsem, asem, a2sem, qsem, dsem, xsem, x2sem, hsem, h2sem, bsem, fsem, ssem):
     s, t = lax.axis_index("sp"), lax.axis_index("tp")
     n_z = n_sp // group
     z, w = s // group, lax.rem(s, group)
@@ -425,7 +381,7 @@
 
     loads = [
         pltpu.make_async_copy(a, b, wsem.at[i])
-        for i, (a, b) in enumerate(((out_w, oc), (gate_h, gate_w), (up_h, up_w), (down_h, down_w)))
+        for i, (a, b) in enumerate(((gate_h, gate_w), (up_h, up_w)))
     ]
     for load in loads:
         load.start()
@@ -453,29 +409,24 @@
     def left(ref, sem):
         remote(ref, ref, sem, dsem.at[0], s, side(1)).wait_send()
 
-    barrier = pltpu.get_barrier_semaphore()
-
-    def hello(sp, tp):
-        pl.semaphore_signal(barrier, inc=1, device_id=(sp, tp), device_id_type=MESH)
-
-    def greet(o, c):
-        hello(lax.rem(s + o, n_sp), t)
-        return c
-
-    lax.fori_loop(1, n_sp, greet, 0)
-    for d in range(1, n_tp):
-        hello(s, side(d))
     low = t < n_tp // 2
-
-    @pl.when(jnp.logical_not(low))
-    def _():
-        for d in range(n_tp):
-            hello(far_s, d)
-
-    pl.semaphore_wait(barrier, n_sp - 1 + n_tp - 1 + n_tp // 2)
 
     for k, d in enumerate((1, -1)):
         remote(heads, hall.at[t], sent.at[6], asem.at[k], s, side(d)).start()
+
+    sp_home = jnp.where(low, s, far_s)
+    slab = stream_in.at[pl.ds(pl.multiple_of(t * block, block), block)]
+    for q in range(n_tp):
+        piece = rows_in.at[:, pl.ds(q * feats, feats)]
+        at_home = (t == q) & low
+
+        @pl.when(at_home)
+        def _():
+            pltpu.make_async_copy(piece, slab, local_sem.at[3]).start()
+
+        @pl.when(jnp.logical_not(at_home))
+        def _():
+            remote(piece, slab, sent.at[10], ssem.at[t], sp_home, q).start()
 
     base = jnp.concatenate([jnp.concatenate([meta[q]] * 16, axis=0).T[:block] for q in range(n_tp)], axis=0)
     lane = lax.broadcasted_iota(jnp.int32, (rows, 128), 1)
@@ -491,14 +442,13 @@
         places = jnp.where(lane == k, base[:, k : k + 1] * cap + rank, places)
     slots_col[...] = places
     slots_row[...] = places.T[:8]
-    loads[0].wait()
 
     width = heads.shape[1]
 
     def project(x, q):
         return jnp.dot(x, oc[pl.ds(pl.multiple_of(q * width, width), width)], preferred_element_type=f32)
 
-    stream[...] = stream_in[...].astype(f32) + project(heads[...], t)
+    stream[...] = project(heads[...], t)
     for k, d in enumerate((-1, 1)):
         arrived(hall.at[side(d)], asem.at[k])
         ref = hall.at[side(d), pl.ds(k * half, half)]
@@ -506,7 +456,19 @@
     stream[...] += project(hall[side(-1)], side(-1)) + project(hall[side(1)], side(1))
     for k in range(2):
         arrived(hall.at[side(2), pl.ds(k * half, half)], a2sem.at[k])
-    total = stream[...] + project(hall[side(2)], side(2))
+    for q in range(n_tp):
+        ref = stream_in.at[pl.ds(q * block, block)]
+        at_home = (t == q) & low
+
+        @pl.when(at_home)
+        def _():
+            pltpu.make_async_copy(rows_in.at[:, pl.ds(q * feats, feats)], ref, local_sem.at[3]).wait()
+
+        @pl.when(jnp.logical_not(at_home))
+        def _():
+            arrived(ref, ssem.at[q])
+
+    total = stream[...] + project(hall[side(2)], side(2)) + stream_in[...].astype(f32)
     stream[...] = total
 
     part = jnp.sum(total * total, axis=1, keepdims=True)
@@ -554,7 +516,7 @@
         return lax.fori_loop(0, group, one, c)
 
     lax.fori_loop(1, n_z, far, 0)
-    for load in loads[1:]:
+    for load in loads:
         load.wait()
 
     def chunk(q, j):
@@ -702,63 +664,98 @@
     @pl.when(low)
     def _():
         left(mix.at[pl.ds(0, (n_tp - 1) * block)], sent.at[9])
+        left(mix.at[pl.ds(0, (n_tp - 1) * block)], sent.at[10])
 
     @pl.when(jnp.logical_not(low))
     def _():
         left(mix, sent.at[9])
-
-
-def post(heads, out_w, stream_in, gain, meta, gate_w, up_w, down_w, n_sp, n_tp, group, cap):
-    rows, feats = stream_in.shape
-    units = gate_w.shape[1]
-    n_z = n_sp // group
+        left(mix, sent.at[10])
+
+
+def layer_kernel(dims, queries_one, queries_two, keys_one, keys_two, values, meta_in, out_w, down_w, lam, head_gain,
+                 rows_in, norm_gain, gate_h, up_h, out, heads, meta, oc, down, *rest):
+    attention_part(
+        dims, queries_one, queries_two, keys_one, keys_two, values, meta_in, out_w, down_w, lam, head_gain,
+        heads, meta, oc, down, *rest[:N_FRONT],
+    )
+    n_z, n_y, n_c, n_tp, _ = dims
+    stream_in, hall, slots_row, slots_col, gate_w, up_w, *tail = rest[N_FRONT:]
+    experts_part(
+        n_z * n_y * n_c, n_tp, n_y * n_c, heads, rows_in, norm_gain, meta, gate_h, up_h,
+        out, stream_in, hall, slots_row, slots_col, oc, gate_w, up_w, down, *tail,
+    )
+
+
+def layer(queries_one, queries_two, keys_one, keys_two, values, meta, out_w, down_w, lam, head_gain,
+          rows_in, norm_gain, gate_w, up_w, dims):
+    n_z, n_y, n_c, n_tp, split = dims
+    n_sp, group = n_z * n_y * n_c, n_y * n_c
+    rows = queries_one.shape[0]
+    feats = out_w.shape[1] // n_tp
+    units, cap = gate_w.shape[1], CAP
+    turn = n_z // 2
     bf, f32 = jnp.bfloat16, jnp.float32
     dma = pltpu.SemaphoreType.DMA
     vmem, hbm = pl.BlockSpec(memory_space=pltpu.VMEM), pl.BlockSpec(memory_space=pl.ANY)
+    smem = pl.BlockSpec(memory_space=pltpu.SMEM)
+    first = [
+        pltpu.VMEM((n_z, n_y, n_c, rows, 2 * HEAD_DIM + VAL_DIM), bf),
+        pltpu.VMEM((2, rows // 2, 2 * HEAD_DIM), bf),
+        pltpu.VMEM((2, 2, rows, HEAD_DIM), bf),
+        pltpu.VMEM((2, 2, rows, 128), f32),
+        pltpu.VMEM((2, 2, rows, 128), f32),
+        pltpu.VMEM((2, 2, rows, VAL_DIM), f32),
+        dma((12,)), dma((7,)), dma((2,)), dma((n_tp,)), dma((n_tp,)), dma((n_tp,)),
+        dma((2, turn + 1)), dma((n_z, 2)), dma((n_z,)), dma((2,)), dma((1,)), dma((4, 2, turn + 1)), dma((n_z,)),
+    ]
+    assert len(first) == N_FRONT
+    second = [
+        pltpu.VMEM((rows, feats), bf),
+        pltpu.VMEM((n_tp, rows, 2 * VAL_DIM), bf),
+        pltpu.VMEM((8, rows), f32),
+        pltpu.VMEM((rows, 128), f32),
+        pltpu.VMEM(gate_w.shape, bf),
+        pltpu.VMEM(up_w.shape, bf),
+        pltpu.VMEM((rows, feats), f32),
+        pltpu.VMEM((n_tp, 8, rows), f32),
+        pltpu.VMEM((n_sp, cap, feats), bf),
+        pltpu.VMEM((n_tp, n_sp, cap, feats), bf),
+        pltpu.VMEM((n_tp, n_z, group * cap, units), bf),
+        pltpu.VMEM((n_sp, cap, feats), bf),
+        pltpu.VMEM((n_sp, cap, feats), bf),
+        pltpu.VMEM((rows, feats), bf),
+        dma((11,)), dma((4,)), dma((4,)), dma((2,)), dma((2,)), dma((n_tp,)), dma((n_z,)), dma((2, n_z)),
+        dma((n_z,)), dma((2, n_z)), dma((n_z,)), dma((n_z,)), dma((n_tp,)), dma((n_tp,)),
+    ]
     return pl.pallas_call(
-        functools.partial(post_kernel, n_sp, n_tp, group),
+        functools.partial(layer_kernel, dims),
         out_shape=jax.ShapeDtypeStruct((rows // n_tp, feats * n_tp), bf),
-        in_specs=[vmem, hbm, vmem, vmem, vmem, hbm, hbm, hbm],
+        in_specs=[vmem, vmem, hbm, hbm, hbm, vmem, hbm, hbm, smem, vmem, vmem, vmem, hbm, hbm],
         out_specs=vmem,
         scratch_shapes=[
-            pltpu.VMEM((n_tp,) + heads.shape, bf),
-            pltpu.VMEM((8, rows), f32),
-            pltpu.VMEM((rows, 128), f32),
-            pltpu.VMEM(out_w.shape, bf),
-            pltpu.VMEM(gate_w.shape, bf),
-            pltpu.VMEM(up_w.shape, bf),
-            pltpu.VMEM(down_w.shape, bf),
-            pltpu.VMEM((rows, feats), f32),
-            pltpu.VMEM((n_tp, 8, rows), f32),
-            pltpu.VMEM((n_sp, cap, feats), bf),
-            pltpu.VMEM((n_tp, n_sp, cap, feats), bf),
-            pltpu.VMEM((n_tp, n_z, group * cap, units), bf),
-            pltpu.VMEM((n_sp, cap, feats), bf),
-            pltpu.VMEM((n_sp, cap, feats), bf),
-            pltpu.VMEM((rows, feats), bf),
-            dma((10,)), dma((3,)), dma((4,)), dma((2,)), dma((2,)), dma((n_tp,)), dma((n_z,)), dma((2, n_z)),
-            dma((n_z,)), dma((2, n_z)), dma((n_z,)), dma((n_z,)), dma((n_tp,)),
-        ],
+            pltpu.VMEM((rows, 2 * VAL_DIM), bf),
+            pltpu.VMEM((n_tp,) + meta.shape, f32),
+            pltpu.VMEM((n_tp * out_w.shape[0], feats), bf),
+            pltpu.VMEM((n_tp * down_w.shape[0], feats), bf),
+        ]
+        + first
+        + second,
         compiler_params=pltpu.CompilerParams(
-            collective_id=1, has_side_effects=True, vmem_limit_bytes=60 * 1024 * 1024),
-        name="post",
-    )(heads, out_w, stream_in, gain, meta, gate_w, up_w, down_w)
+            collective_id=0, has_side_effects=True, vmem_limit_bytes=60 * 1024 * 1024),
+        name="layer",
+    )(queries_one, queries_two, keys_one, keys_two, values, meta, out_w, down_w, lam, head_gain,
+      rows_in, norm_gain, gate_w, up_w)
 
 
 def shards(
     stream_in, queries_one, queries_two, keys_one, keys_two, values, lambdas, head_gain, out_weight,
     norm_gain, expert_ids, route_weight, gate_weight, up_weight, down_weight,
 ):
-    n_sp, n_tp = lax.axis_size("sp"), lax.axis_size("tp")
     meta = jnp.concatenate([expert_ids.astype(jnp.float32), route_weight], 1).T
     meta = jnp.pad(meta, ((0, 8 - meta.shape[0]), (0, 128 - meta.shape[1])))
-    heads, stream, meta, out_cols, down_cols = front(
-        queries_one, queries_two, keys_one, keys_two, values, stream_in, meta, out_weight, down_weight[0],
-        lambdas, head_gain[None], CHIPS + (n_tp, SPLIT),
-    )
-    return post(
-        heads, out_cols, stream, norm_gain[None], meta, gate_weight[0], up_weight[0], down_cols,
-        n_sp, n_tp, n_sp // CHIPS[0], CAP,
+    return layer(
+        queries_one, queries_two, keys_one, keys_two, values, meta, out_weight, down_weight[0], lambdas, head_gain[None],
+        stream_in, norm_gain[None], gate_weight[0], up_weight[0], CHIPS + (lax.axis_size("tp"), SPLIT),
     )
 
 

time: 201 us -> 192 us (0.955); the launches traced: 201 us -> 189 us
  Pallas kernels: 197 us -> 186 us
    pallas_call x2 -> x1, Pallas kernels: 197 us -> 186 us  [layer(): pl.pallas_call(functools.partial(layer_kernel, dims), out_shape=jax.Shape...]
where the time goes in v5:
time: 192 us; the launch traced here: 189 us
  Pallas kernels  186 us (97%)
  local copies, waits for them, and re-layouts  2.27 us (1%)
    pallas_call x1, Pallas kernels, layer(): pl.pallas_call(functools.partial(layer_kernel, dims), out_shape=jax.Shape...  186 us

profile of v5, /device:TPU:7, one launch (start us, length us, event | category | flops | bytes accessed | tf_op | source)
XLA Modules:
  0.0 189.2 jit_solution(14855987157203061394)
XLA Ops:
  0.0 0.7 convert_element_type.5
  0.7 0.7 maximum_bitcast_fusion
  1.4 0.6 pad.4.meta_in
  2.0 185.6 %layer.1 = bf16[64,2048]{1,0:T(8,128)(2,1)} custom-call(bf16[256,256]{1,0:T(8,128)(2,1)} %queries_one.1, bf16[256,256]{1,0:T(8,128)(2,1)} %queries_two.1, bf16[256,128]{1,0:T(8,128)(2,1)} %keys_one.1, bf16[256,128]{1,0:T(8,128)(2,1)} %keys_two.1, bf16[256,256]{1,0:T(8,128)(2,1)} %values.1, f32[8,128]{1,0:T(8,128)} %pad.4.meta_in, bf16[512,2048]{1,0:T(8,128)(2,1)} %out_w.1, ...), custom_call_target="tpu_custom_call" | custom-call | tf_op jit(solution)/shard_map/layer/pallas_call | solution.py:730
  187.5 1.7 copy.17

commit v6 on v5

--- a/solution.py
+++ b/solution.py
@@ -21,7 +21,7 @@
 N_FRONT = 19
 
 
-def attention_part(dims, queries_one, queries_two, keys_one, keys_two, values, meta_in, out_w, down_w, lam, gain,
+def attention_part(dims, late, queries_one, queries_two, keys_one, keys_two, values, meta_in, out_w, down_w, lam, gain,
                  heads, meta, out_cols, down_cols, kv, q_far, q_all, m_ref, l_ref, acc_ref,
                  sent, local_sem, qsem, msem, osem, wsem, pz, py, py2, ry, ry2, rz, sib):
     n_z, n_y, n_c, n_tp, split = dims
@@ -311,6 +311,10 @@
                     q_all[0, i, place] = queries[:half, lanes]
                     q_all[1, i, place] = q_far[i, :, lanes]
 
+        @pl.when(u == 5 * turn + 6)
+        def _():
+            late()
+
         return attend(done, u)
 
     lax.fori_loop(5, 5 * turn + LAST, step, jnp.int32(0))
@@ -414,20 +418,6 @@
     for k, d in enumerate((1, -1)):
         remote(heads, hall.at[t], sent.at[6], asem.at[k], s, side(d)).start()
 
-    sp_home = jnp.where(low, s, far_s)
-    slab = stream_in.at[pl.ds(pl.multiple_of(t * block, block), block)]
-    for q in range(n_tp):
-        piece = rows_in.at[:, pl.ds(q * feats, feats)]
-        at_home = (t == q) & low
-
-        @pl.when(at_home)
-        def _():
-            pltpu.make_async_copy(piece, slab, local_sem.at[3]).start()
-
-        @pl.when(jnp.logical_not(at_home))
-        def _():
-            remote(piece, slab, sent.at[10], ssem.at[t], sp_home, q).start()
-
     base = jnp.concatenate([jnp.concatenate([meta[q]] * 16, axis=0).T[:block] for q in range(n_tp)], axis=0)
     lane = lax.broadcasted_iota(jnp.int32, (rows, 128), 1)
     earlier = lax.broadcasted_iota(jnp.int32, (rows, rows), 1) < lax.broadcasted_iota(jnp.int32, (rows, rows), 0)
@@ -672,14 +662,37 @@
         left(mix, sent.at[10])
 
 
+def send_stream(n_sp, n_tp, rows_in, stream_in, sent, local_sem, ssem):
+    s, t = lax.axis_index("sp"), lax.axis_index("tp")
+    far_s, low = n_sp - 1 - s, t < n_tp // 2
+    block, feats = rows_in.shape[0], stream_in.shape[1]
+    sp_home = jnp.where(low, s, far_s)
+    slab = stream_in.at[pl.ds(pl.multiple_of(t * block, block), block)]
+    for q in range(n_tp):
+        piece = rows_in.at[:, pl.ds(q * feats, feats)]
+        at_home = (t == q) & low
+
+        @pl.when(at_home)
+        def _():
+            pltpu.make_async_copy(piece, slab, local_sem.at[3]).start()
+
+        @pl.when(jnp.logical_not(at_home))
+        def _():
+            pltpu.make_async_remote_copy(
+                src_ref=piece, dst_ref=slab, send_sem=sent.at[10], recv_sem=ssem.at[t], device_id=(sp_home, q),
+                device_id_type=MESH).start()
+
+
 def layer_kernel(dims, queries_one, queries_two, keys_one, keys_two, values, meta_in, out_w, down_w, lam, head_gain,
                  rows_in, norm_gain, gate_h, up_h, out, heads, meta, oc, down, *rest):
+    n_z, n_y, n_c, n_tp, _ = dims
+    stream_in, hall, slots_row, slots_col, gate_w, up_w, *tail = rest[N_FRONT:]
+    late = functools.partial(
+        send_stream, n_z * n_y * n_c, n_tp, rows_in, stream_in, tail[8], tail[9], tail[-1])
     attention_part(
-        dims, queries_one, queries_two, keys_one, keys_two, values, meta_in, out_w, down_w, lam, head_gain,
+        dims, late, queries_one, queries_two, keys_one, keys_two, values, meta_in, out_w, down_w, lam, head_gain,
         heads, meta, oc, down, *rest[:N_FRONT],
     )
-    n_z, n_y, n_c, n_tp, _ = dims
-    stream_in, hall, slots_row, slots_col, gate_w, up_w, *tail = rest[N_FRONT:]
     experts_part(
         n_z * n_y * n_c, n_tp, n_y * n_c, heads, rows_in, norm_gain, meta, gate_h, up_h,
         out, stream_in, hall, slots_row, slots_col, oc, gate_w, up_w, down, *tail,

time: 192 us -> 190 us (0.990)
  Pallas kernels: 186 us -> 184 us
where the time goes in v6:
time: 190 us; the launch traced here: 188 us
  Pallas kernels  184 us (97%)
  local copies, waits for them, and re-layouts  2.27 us (1%)
    pallas_call x1, Pallas kernels, layer(): pl.pallas_call(functools.partial(layer_kernel, dims), out_shape=jax.Shape...  184 us

profile of v6, /device:TPU:7, one launch (start us, length us, event | category | flops | bytes accessed | tf_op | source)
XLA Modules:
  0.0 187.8 jit_solution(7079379823740177385)
XLA Ops:
  0.0 0.7 convert_element_type.5
  0.7 0.7 maximum_bitcast_fusion
  1.4 0.6 pad.4.meta_in
  2.0 184.1 %layer.1 = bf16[64,2048]{1,0:T(8,128)(2,1)} custom-call(bf16[256,256]{1,0:T(8,128)(2,1)} %queries_one.1, bf16[256,256]{1,0:T(8,128)(2,1)} %queries_two.1, bf16[256,128]{1,0:T(8,128)(2,1)} %keys_one.1, bf16[256,128]{1,0:T(8,128)(2,1)} %keys_two.1, bf16[256,256]{1,0:T(8,128)(2,1)} %values.1, f32[8,128]{1,0:T(8,128)} %pad.4.meta_in, bf16[512,2048]{1,0:T(8,128)(2,1)} %out_w.1, ...), custom_call_target="tpu_custom_call" | custom-call | tf_op jit(solution)/shard_map/layer/pallas_call | solution.py:743
  186.1 1.7 copy.17
